TPU v7x, 128 devices: a whole 4x4x4 slice. The times are simulated.
128 devices in a mesh: fs: 16 (over z, y), tp: 8 (over x, core).
Axes of the slice: x: 4, y: 4, z: 4, core: 2. Of those that a mesh axis runs over, the one named last changes fastest.
Arguments:
- saved_input: bfloat16 [196608, 2048], P(('fs', 'tp')), may hold values from -6 to 6
- key_cot: bfloat16 [196608, 1024], P(('fs', 'tp')), may hold values from -0.020184243 to 0.020184243
- mixed_out: bfloat16 [196608, 1024], P(('fs', 'tp')), may hold values from -6 to 6
- out_cot: bfloat16 [196608, 2048], P(('fs', 'tp')), may hold values from -0.020184243 to 0.020184243
- key_weight: float32 [2048, 1024], P('fs', 'tp'), may hold values from -0.125 to 0.125
- out_weight: float32 [1024, 2048], P('tp', 'fs'), may hold values from -0.1875 to 0.1875
- bases: bfloat16 [2, 1024, 512], replicated, may hold values from -0.1875 to 0.1875
- first_moment: float32 [2, 2048, 512], P(None, 'fs', 'tp'), may hold values from -64 to 64
- second_moment: float32 [2, 2048, 512], P(None, 'fs', 'tp'), may hold values from 0.25 to 4
Outputs:
- key_weight_new: float32 [2048, 1024], P('fs', 'tp')
- out_weight_new: float32 [1024, 2048], P('tp', 'fs')
- key_step: float32 [2048, 1024], P('fs', 'tp')
- out_step: float32 [1024, 2048], P('tp', 'fs')
- first_new: float32 [2, 2048, 512], P(None, 'fs', 'tp')
- second_new: float32 [2, 2048, 512], P(None, 'fs', 'tp')
- key_copy: bfloat16 [2048, 1024], P(None, 'tp')
- out_copy: bfloat16 [1024, 2048], P('tp')
All inputs are finite; a program needn't handle non-finite values.
Results may differ from a plain program's by a relative error of at most 0.0032.
Values may be sent and summed in bfloat16 or wider, within the bound.
No kernel may reach another device: no remote copies, remote signals or barrier semaphores. Data moves between devices by JAX's collectives and lax.ppermute only.
A program may use at most 128 MiB of HBM per device.

v0:
```python
import functools

import jax
import jax.numpy as jnp
from jax import lax
from jax.experimental import pallas as pl
from jax.experimental.pallas import tpu as pltpu
from jax.sharding import Mesh
from jax.sharding import PartitionSpec as P

D = 2048
RANK = 512
FS = ("fs_0", "fs_1")
TP = ("tp_0", "tp_1")
CHIPS = ("fs_0", "tp_0", "fs_1")
ROWS_AND_CORE = ("tp_1", "fs_0", "fs_1")
FS_TP = ("fs_0", "fs_1", "tp_0", "tp_1")
SWAP = [(0, 1), (1, 0)]
LANES = 128
MIB = 2**20


first_decay = 0.8
second_decay = 0.9
learn_rate = 0.01

wide = jnp.float32
narrow = jnp.bfloat16
in_smem = pl.BlockSpec(memory_space=pltpu.SMEM)
in_hbm = pl.BlockSpec(memory_space=pltpu.HBM)
in_vmem = pl.BlockSpec(memory_space=pltpu.VMEM)


def exchanged(tiles, axes):
    return lax.all_to_all(tiles, axes, split_axis=0, concat_axis=0, tiled=True)


def swapped(array):
    return lax.ppermute(array, "tp_1", SWAP)


def pick(core, zero, one):
    return jnp.where(core == 0, zero, one)


PARTS = 3
CHUNKS = 8


def map_part(i, cols, base, mapped):
    part = cols.shape[0] // PARTS
    at = pl.ds(i * part, part)
    block = jnp.dot(cols[at, :], base[...], preferred_element_type=wide)
    mapped[:, at] = block.astype(narrow).T


def contract(mapped, rows, out):
    chunk = out.shape[1] // CHUNKS
    for j in range(CHUNKS):
        at = pl.ds(j * chunk, chunk)
        total, start = (None, 0)
        for piece in rows:
            length = piece.shape[0]
            block = jnp.dot(
                mapped[:, start : start + length], piece[:, at], preferred_element_type=wide
            )
            total = block if total is None else total + block
            start += length
        out[:, at] = total.astype(out.dtype)


def partner_kernel(
    core, rows0, cols0, rows1, cols1, bases, out, rows2, cols2, base2, rows, cols, base, mapped, sems
):
    part = cols.shape[0] // PARTS
    early = rows2.shape[0]

    def base_load(k):
        matrix = core[0] if k else 1 - core[0]
        return pltpu.make_async_copy(bases.at[matrix], (base, base2)[k], sems.at[k])

    def cols_load(source, i):
        at = pl.ds(i * part, part)
        return pltpu.make_async_copy(source.at[at], cols.at[at], sems.at[2 + i])

    def rows_load(source):
        return pltpu.make_async_copy(source, rows, sems.at[5])

    def own_cols_load(source):
        return pltpu.make_async_copy(source, cols2, sems.at[6])

    def own_rows_load(source):
        return pltpu.make_async_copy(source.at[pl.ds(0, early)], rows2, sems.at[7])

    def start(zero, load, first, second):
        @pl.when(core[0] == zero)
        def _():
            load(first).start()

        @pl.when(core[0] != zero)
        def _():
            load(second).start()

    base_load(0).start()
    for i in range(PARTS):
        start(1, lambda source, i=i: cols_load(source, i), cols0, cols1)
    base_load(0).wait()
    for i in range(PARTS):
        cols_load(cols0, i).wait()
        if i == 0:
            start(1, rows_load, rows0, rows1)
        map_part(i, cols, base, mapped)
    rows_load(rows0).wait()
    base_load(1).start()
    start(0, own_cols_load, cols0, cols1)
    start(0, own_rows_load, rows0, rows1)
    contract(mapped, (rows,), out)
    base_load(1).wait()
    own_cols_load(cols0).wait()
    own_rows_load(rows0).wait()


def own_kernel(core, rows0, rows1, rows, cols, base, out, late, mapped, sem):
    def late_load(source):
        return pltpu.make_async_copy(source.at[pl.ds(rows.shape[0], late.shape[0])], late, sem)

    @pl.when(core[0] == 0)
    def _():
        late_load(rows0).start()

    @pl.when(core[0] != 0)
    def _():
        late_load(rows1).start()

    for i in range(PARTS):
        map_part(i, cols, base, mapped)
    late_load(rows0).wait()
    contract(mapped, (rows, late), out)


def cost_of(tokens, height, width, rank):
    return pl.CostEstimate(
        flops=2 * tokens * rank * (height + width),
        bytes_accessed=2 * tokens * (height + width),
        transcendentals=0,
    )


def both_low(core, saved_input, key_cot, out_cot, mixed_out, bases):
    tokens, height = saved_input.shape
    _, width, rank = bases.shape
    early = tokens // 2
    cost = cost_of(tokens, height, width, rank)
    rows0, cols0, rows1, cols1, in_bases = (
        pltpu.with_memory_space_constraint(a, pltpu.HBM)
        for a in (saved_input, key_cot, out_cot, mixed_out, bases)
    )
    theirs, rows, cols, base = pl.pallas_call(
        partner_kernel,
        out_shape=(
            pltpu.VMEM((rank, height), narrow),
            pltpu.VMEM((early, height), narrow),
            pltpu.VMEM((tokens, width), narrow),
            pltpu.VMEM((width, rank), narrow),
        ),
        in_specs=[in_smem] + [in_hbm] * 5,
        out_specs=(in_vmem,) * 4,
        scratch_shapes=[
            pltpu.VMEM((tokens, height), narrow),
            pltpu.VMEM((tokens, width), narrow),
            pltpu.VMEM((width, rank), narrow),
            pltpu.VMEM((rank, tokens), narrow),
            pltpu.SemaphoreType.DMA((8,)),
        ],
        compiler_params=pltpu.CompilerParams(vmem_limit_bytes=20 * MIB),
        cost_estimate=cost,
        name="partner_low",
    )(core, rows0, cols0, rows1, cols1, in_bases)
    from_partner = swapped(theirs)
    mine = pl.pallas_call(
        own_kernel,
        out_shape=pltpu.VMEM((rank, height), wide),
        in_specs=[in_smem] + [in_hbm] * 2 + [in_vmem] * 3,
        out_specs=in_vmem,
        scratch_shapes=[
            pltpu.VMEM((tokens - early, height), narrow),
            pltpu.VMEM((rank, tokens), narrow),
            pltpu.SemaphoreType.DMA,
        ],
        compiler_params=pltpu.CompilerParams(vmem_limit_bytes=14 * MIB),
        cost_estimate=cost,
        name="own_low",
    )(core, rows0, rows1, rows, cols, base)
    return mine, from_partner


def combine_kernel(mine, partner, out, tiles, sems, *, n_x, n_y):
    count = out.shape[0] // sems.shape[0]
    for z in range(sems.shape[0]):
        for x in range(n_x):
            for y in range(n_y):
                ranks, rows = (pl.ds(x * LANES, LANES), pl.ds((z * n_y + y) * LANES, LANES))
                total = mine[ranks, rows] + partner[ranks, rows].astype(wide)
                tiles[(z * n_x + x) * n_y + y] = total.astype(narrow)
        at = pl.ds(z * count, count)
        pltpu.make_async_copy(tiles.at[at], out.at[at], sems.at[z]).start()
    for z in range(sems.shape[0]):
        at = pl.ds(z * count, count)
        pltpu.make_async_copy(tiles.at[at], out.at[at], sems.at[z]).wait()


def combine(mine, partner, n_z, n_y, n_x):
    shape = (n_z * n_y * n_x, LANES, LANES)
    return pl.pallas_call(
        functools.partial(combine_kernel, n_x=n_x, n_y=n_y),
        out_shape=pltpu.HBM(shape, narrow),
        in_specs=[in_vmem] * 2,
        out_specs=in_hbm,
        scratch_shapes=[pltpu.VMEM(shape, narrow), pltpu.SemaphoreType.DMA((n_z,))],
        compiler_params=pltpu.CompilerParams(vmem_limit_bytes=8 * MIB),
        name="combine",
    )(mine, partner)


def moments_kernel(core, low, firsts, seconds, got, first, second, direction):
    zero = core[0] == 0

    def joined(old, came):
        kept = jnp.where(zero, old[0], old[1])
        return jnp.concatenate((jnp.where(zero, kept, came), jnp.where(zero, came, kept)), axis=0)

    sums = low[...]
    first_new = first_decay * joined(firsts, got[0]) + (1.0 - first_decay) * sums
    second_new = second_decay * joined(seconds, got[1]) + (1.0 - second_decay) * sums * sums
    first[...] = first_new
    second[...] = second_new
    direction[...] = first_new / jnp.sqrt(second_new)


def new_moments(core, low, firsts, seconds, got):
    return pl.pallas_call(
        moments_kernel,
        out_shape=(pltpu.VMEM(low.shape, wide),) * 3,
        in_specs=[in_smem] + [in_vmem] * 4,
        out_specs=(in_vmem,) * 3,
        compiler_params=pltpu.CompilerParams(vmem_limit_bytes=4 * MIB),
        name="moments",
    )(core, low, firsts, seconds, got)


def project_kernel(where, bases, *refs):
    *directions, own, other, row, base, sem = refs
    core, chip_x = (where[0], where[1])
    cols = own.shape[0]
    n_x = len(directions)
    at = pl.ds(pl.multiple_of(chip_x * 2 * cols, 2 * cols), 2 * cols)
    load = pltpu.make_async_copy(bases.at[core, at], base, sem)
    load.start()
    square = jnp.zeros((1, LANES), wide)
    parts = []
    for x in range(n_x):
        part = directions[0][...]
        back = lax.rem(chip_x - x + n_x, n_x)
        for s in range(1, n_x):
            part = jnp.where(back == s, directions[s][...], part)
        square = square + jnp.sum(part * part, axis=0, keepdims=True)
        parts.append(part)
    square = jnp.sum(square, axis=1, keepdims=True)
    lanes = lax.broadcasted_iota(jnp.int32, (1, LANES), 1)
    row[...] = jnp.broadcast_to(jnp.where(lanes == core, square, 0.0)[None], row.shape)
    load.wait()
    total = jnp.zeros((2 * cols, parts[0].shape[1]), wide)
    for x, part in enumerate(parts):
        width, n = part.shape
        high = part.astype(narrow)
        rest = part - high.astype(wide)
        middle = rest.astype(narrow)
        low = (rest - middle.astype(wide)).astype(narrow)
        limbs = jnp.concatenate((high, middle, low), axis=1)
        product = jnp.dot(
            base[:, x * width : (x + 1) * width], limbs, preferred_element_type=wide
        )
        total = total + (product[:, :n] + (product[:, n : 2 * n] + product[:, 2 * n :]))
    left, right = (total[:cols], total[cols:])
    own[...] = jnp.where(core == 0, left, right)
    other[...] = jnp.where(core == 0, right, left)


def project(where, bases, directions, cols, peers):
    out = pltpu.VMEM((cols, directions[0].shape[1]), wide)
    return pl.pallas_call(
        project_kernel,
        out_shape=(out, out, jax.ShapeDtypeStruct((peers, 1, LANES), wide)),
        in_specs=[in_smem, in_hbm] + [in_vmem] * len(directions),
        out_specs=(in_vmem,) * 3,
        scratch_shapes=[
            pltpu.VMEM((2 * cols, bases.shape[2]), narrow),
            pltpu.SemaphoreType.DMA,
        ],
        compiler_params=pltpu.CompilerParams(vmem_limit_bytes=6 * MIB),
        name="project",
    )(where, bases, *directions)


def steps_of(core, sums, own, came, key_weight, out_weight):
    total = jnp.sum(sums[...], axis=0)
    scales = lax.rsqrt(total / (D * RANK) + 1.0)
    lanes = lax.broadcasted_iota(jnp.int32, scales.shape, 1)
    key_scale = jnp.sum(jnp.where(lanes == 0, scales, 0.0), axis=1, keepdims=True)
    out_scale = jnp.sum(jnp.where(lanes == 1, scales, 0.0), axis=1, keepdims=True)
    zero = core[0] == 0
    key_step = jnp.where(zero, own[...], came[...]).T * key_scale
    out_step = jnp.where(zero, came[...], own[...]) * out_scale
    key_new = key_weight[...] - learn_rate * key_step
    out_new = out_weight[...] - learn_rate * out_step
    return (key_new, out_new, key_step, out_step)


def copies_kernel(core, sums, own, came, key_weight, out_weight, copies):
    key_new, out_new, _, _ = steps_of(core, sums, own, came, key_weight, out_weight)
    copies[...] = jnp.broadcast_to(
        jnp.stack((key_new.astype(narrow), out_new.astype(narrow)))[None], copies.shape
    )


def steps_kernel(core, sums, own, came, key_weight, out_weight, *outs):
    for out, value in zip(outs, steps_of(core, sums, own, came, key_weight, out_weight)):
        out[...] = value


def stepped(kernel, outs, *args):
    return pl.pallas_call(
        kernel,
        out_shape=outs,
        in_specs=[in_smem] + [in_vmem] * 5,
        out_specs=jax.tree.map(lambda _: in_vmem, outs),
        compiler_params=pltpu.CompilerParams(vmem_limit_bytes=6 * MIB),
    )(*args)


def spread_kernel(gathered, key_copy, out_copy, *, n_y):
    n_z = gathered.shape[0] // n_y
    for y in range(n_y):
        for z in range(n_z):
            at = pl.ds((z * n_y + y) * LANES, LANES)
            key_copy[at, :] = gathered[y * n_z + z, 0]
            out_copy[:, at] = gathered[y * n_z + z, 1]


def spread(gathered, n_y):
    n_fs, _, rows, cols = gathered.shape
    return pl.pallas_call(
        functools.partial(spread_kernel, n_y=n_y),
        out_shape=(
            jax.ShapeDtypeStruct((n_fs * rows, cols), narrow),
            jax.ShapeDtypeStruct((cols, n_fs * rows), narrow),
        ),
        in_specs=[in_vmem],
        out_specs=(in_vmem, in_vmem),
        compiler_params=pltpu.CompilerParams(vmem_limit_bytes=6 * MIB),
        name="spread",
    )(gathered)


def body(
    saved_input,
    key_cot,
    mixed_out,
    out_cot,
    key_weight,
    out_weight,
    bases,
    first_moment,
    second_moment,
):
    core = lax.axis_index("tp_1").astype(jnp.int32)
    chip_x = lax.axis_index("tp_0").astype(jnp.int32)
    n_z, n_y, n_x = (lax.axis_size(axis) for axis in ("fs_0", "fs_1", "tp_0"))
    rows, cols = key_weight.shape
    half = first_moment.shape[2]
    this = core.reshape(1)

    mine, from_partner = both_low(this, saved_input, key_cot, out_cot, mixed_out, bases)
    arrived = exchanged(combine(mine, from_partner, n_z, n_y, n_x), CHIPS)
    low = arrived.astype(wide).sum(axis=0)

    firsts = first_moment.transpose(0, 2, 1)
    seconds = second_moment.transpose(0, 2, 1)
    got = swapped(
        jnp.stack((pick(core, firsts[1], firsts[0]), pick(core, seconds[1], seconds[0])))
    )
    first, second, direction = new_moments(this, low, firsts, seconds, got)

    directions = [direction] + [
        lax.ppermute(direction, "tp_0", [(i, (i + s) % n_x) for i in range(n_x)])
        for s in range(1, n_x)
    ]
    own, other, row = project(
        jnp.stack((core, chip_x)), bases, directions, cols, lax.axis_size(ROWS_AND_CORE)
    )
    sums = exchanged(row, ROWS_AND_CORE)
    came = swapped(other)
    square = jax.ShapeDtypeStruct((rows, cols), wide)
    args = (this, sums, own, came, key_weight, out_weight)
    copies = stepped(copies_kernel, pltpu.HBM((n_z * n_y, 2, rows, cols), narrow), *args)
    gathered = exchanged(copies, ("fs_1", "fs_0"))
    key_new, out_new, key_step, out_step = stepped(steps_kernel, (square,) * 4, *args)
    key_copy, out_copy = spread(gathered, n_y)

    news = jnp.stack((first, second))
    low_half, high_half = (news[:, :half], news[:, half:])
    stay = pick(core, low_half, high_half)
    come = swapped(pick(core, high_half, low_half))
    key_moments = pick(core, stay, come)
    out_moments = pick(core, come, stay)
    first_new = jnp.stack((key_moments[0], out_moments[0])).transpose(0, 2, 1)
    second_new = jnp.stack((key_moments[1], out_moments[1])).transpose(0, 2, 1)
    return (key_new, out_new, key_step, out_step, first_new, second_new, key_copy, out_copy)


def solution(mesh):
    torus = Mesh(mesh.devices.reshape(4, 4, 4, 2), ("fs_0", "fs_1", "tp_0", "tp_1"))
    placed = (
        P(FS_TP, None),
        P(FS_TP, None),
        P(FS_TP, None),
        P(FS_TP, None),
        P(FS, TP),
        P(TP, FS),
        P(),
        P(None, FS, TP),
        P(None, FS, TP),
    )
    return jax.shard_map(
        body,
        mesh=torus,
        in_specs=placed,
        out_specs=(
            P(FS, TP),
            P(TP, FS),
            P(FS, TP),
            P(TP, FS),
            P(None, FS, TP),
            P(None, FS, TP),
            P(None, TP),
            P(TP, None),
        ),
        check_vma=False,
    )
```

profile of v0, /device:TPU:0, one launch (start us, length us, event | category | flops | bytes accessed | tf_op | source)
XLA Modules:
  0.0 103.1 jit_solution(5375900794707761656)
XLA Ops:
  0.6 8.0 %partner_low.1 = (bf16[512,2048]{1,0:T(8,128)(2,1)S(1)}, bf16[768,2048]{1,0:T(8,128)(2,1)S(1)}, bf16[1536,1024]{1,0:T(8,128)(2,1)S(1)}, bf16[1024,512]{1,0:T(8,128)(2,1)S(1)}) custom-call(s32[1]{0:T(128)} %bitcast.core, bf16[1536,2048]{1,0:T(8,128)(2,1)} %rows0.3, bf16[1536,1024]{1,0:T(8,128)(2,1)} %cols0.1, bf16[1536,2048]{1,0:T(8,128)(2,1)} %rows1.3, ...), custom_call_target="tpu_custom_call" | custom-call | flops 4831838208 | bytes 9437184 | tf_op jit(solution)/shard_map/partner_low/pallas_call | solution.py:158
  8.6 0.1 collective-permute-start
  8.7 5.3 %own_low.1.mine = f32[512,2048]{1,0:T(8,128)S(1)} custom-call(s32[1]{0:T(128)} %bitcast.core, bf16[1536,2048]{1,0:T(8,128)(2,1)} %rows0.3, bf16[1536,2048]{1,0:T(8,128)(2,1)} %rows1.3, bf16[768,2048]{1,0:T(8,128)(2,1)S(1)} %get-tuple-element.24.rows, bf16[1536,1024]{1,0:T(8,128)(2,1)S(1)} %get-tuple-element.25.cols, bf16[1024,512]{1,0:T(8,128)(2,1)S(1)} %get-tuple-element.26.base), custom_call_target="tpu_custom_call" | custom-call | flops 4831838208 | bytes 9437184 | tf_op jit(solution)/shard_map/own_low/pallas_call | solution.py:180
  14.1 1.4 %combine.1 = bf16[64,128,128]{2,1,0:T(8,128)(2,1)} custom-call(f32[512,2048]{1,0:T(8,128)S(1)} %own_low.1.mine, bf16[512,2048]{1,0:T(8,128)(2,1)S(1)} %collective-permute-done.partner), custom_call_target="tpu_custom_call" | custom-call | tf_op jit(solution)/shard_map/combine/pallas_call | solution.py:214
  15.5 11.9 %all-to-all-start = ((bf16[64,128,128]{2,1,0:T(8,128)(2,1)}), bf16[64,128,128]{2,1,0:T(8,128)(2,1)}, u32[]{:S(2)}, u32[]{:S(2)}) async-start(bf16[64,128,128]{2,1,0:T(8,128)(2,1)} %combine.1), calls=%async_computation | async-start | bytes 4194304 | tf_op jit(solution)/shard_map/all_to_all | solution.py:35
  27.6 0.3 collective-permute-start.1
  27.9 29.7 %all-to-all-done = bf16[64,128,128]{2,1,0:T(8,128)(2,1)} async-done(((bf16[64,128,128]{2,1,0:T(8,128)(2,1)}), bf16[64,128,128]{2,1,0:T(8,128)(2,1)}, u32[]{:S(2)}, u32[]{:S(2)}) %all-to-all-start) | async-done | bytes 2097184 | tf_op jit(solution)/shard_map/all_to_all | solution.py:35
  57.6 1.9 %convert_reduce_fusion.low = f32[128,128]{1,0:T(8,128)S(1)} fusion(bf16[64,128,128]{2,1,0:T(8,128)(2,1)} %all-to-all-done), kind=kLoop, calls=%fused_computation | loop fusion | flops 2080768 | bytes 2162688 | tf_op jit(solution)/shard_map/reduce_sum | solution.py:385
  59.6 0.7 collective-permute-start.2
  60.2 2.4 %collective-permute-start.3 = (f32[128,128]{1,0:T(8,128)S(1)}, f32[128,128]{1,0:T(8,128)S(1)}, u32[]{:S(2)}, u32[]{:S(2)}) collective-permute-start(f32[128,128]{1,0:T(8,128)S(1)} %get-tuple-element.28.refs_0_), channel_id=1, source_target_pairs={{0,4},{2,6},{4,0},{6,2},{1,5},{3,7},{5,1},{7,3},{8,12},{10,14},{12... | collective-permute-start | bytes 196616 | tf_op jit(solution)/shard_map/ppermute | solution.py:395
  62.7 1.7 %collective-permute-start.4 = (f32[128,128]{1,0:T(8,128)S(1)}, f32[128,128]{1,0:T(8,128)S(1)}, u32[]{:S(2)}, u32[]{:S(2)}) collective-permute-start(f32[128,128]{1,0:T(8,128)S(1)} %get-tuple-element.28.refs_0_), channel_id=1, source_target_pairs={{0,6},{2,0},{4,2},{6,4},{1,7},{3,1},{5,3},{7,5},{8,14},{10,8},{12,... | collective-permute-start | bytes 196616 | tf_op jit(solution)/shard_map/ppermute | solution.py:395
  64.5 0.7 collective-permute-done.2.refs_1_
  65.2 0.8 collective-permute-done.3.refs_2_
  66.0 0.9 collective-permute-done.4.refs_3_
  66.9 1.1 %project.1 = (f32[128,128]{1,0:T(8,128)S(1)}, f32[128,128]{1,0:T(8,128)S(1)}, f32[32,1,128]{2,1,0:T(1,128)S(1)}) custom-call(s32[2]{0:T(128)S(1)} %pad_add_fusion.where, bf16[2,1024,512]{2,1,0:T(8,128)(2,1)S(1)} %copy-done, f32[128,128]{1,0:T(8,128)S(1)} %get-tuple-element.28.refs_0_, f32[128,128]{1,0:T(8,128)S(1)} %collective-permute-done.2.refs_1_, ...), custom_call_target="tpu_custom_call" | custom-call | tf_op jit(solution)/shard_map/project/pallas_call | solution.py:291
  68.1 11.0 %all_to_all.15.sums = f32[32,1,128]{2,1,0:T(1,128)S(1)} all-to-all(f32[32,1,128]{2,1,0:T(1,128)S(1)} %get-tuple-element.29), channel_id=1, replica_groups=mesh['fs_0'=4,'fs_1'=4,'tp_0'=4,'tp_1'=2] {'tp_1','fs_0','fs_1'}, dimensions={0} | all-to-all | bytes 32768 | tf_op jit(solution)/shard_map/all_to_all | solution.py:35
  79.1 1.2 %shard_map.153 = bf16[16,2,128,128]{3,2,1,0:T(8,128)(2,1)} custom-call(s32[1]{0:T(128)} %bitcast.core, f32[32,1,128]{2,1,0:T(1,128)S(1)} %all_to_all.15.sums, f32[128,128]{1,0:T(8,128)S(1)} %get-tuple-element.30.own, f32[128,128]{1,0:T(8,128)S(1)} %collective-permute-done.5.came, f32[128,128]{1,0:T(8,128)S(1)} %copy-done.1, f32[128,128]{1,0:T(8,128)S(1)} %copy-done.2), custom_call_target="tpu_custom_call" | custom-call | tf_op jit(solution)/shard_map/pallas_call | solution.py:332
  80.3 3.7 %all-to-all-start.2 = ((bf16[16,2,128,128]{3,2,1,0:T(8,128)(2,1)}), bf16[16,2,128,128]{3,2,1,0:T(8,128)(2,1)S(1)}, u32[]{:S(2)}, u32[]{:S(2)}) async-start(bf16[16,2,128,128]{3,2,1,0:T(8,128)(2,1)} %shard_map.153), calls=%async_computation.2 | async-start | bytes 2097152 | tf_op jit(solution)/shard_map/all_to_all | solution.py:35
  84.1 1.2 %collective-permute-done.6 = f32[2,64,128]{2,1,0:T(8,128)S(1)} collective-permute-done((f32[2,64,128]{2,1,0:T(8,128)S(1)}, f32[2,64,128]{2,1,0:T(8,128)S(1)}, u32[]{:S(2)}, u32[]{:S(2)}) %collective-permute-start.6) | collective-permute-done | bytes 65568 | tf_op jit(solution)/shard_map/ppermute | solution.py:39
  85.4 0.6 maximum_bitcast_fusion.1
  86.0 0.6 maximum_bitcast_fusion
  86.6 0.8 shard_map.152
  87.5 14.5 %all-to-all-done.2.gathered = bf16[16,2,128,128]{3,2,1,0:T(8,128)(2,1)S(1)} async-done(((bf16[16,2,128,128]{3,2,1,0:T(8,128)(2,1)}), bf16[16,2,128,128]{3,2,1,0:T(8,128)(2,1)S(1)}, u32[]{:S(2)}, u32[]{:S(2)}) %all-to-all-start.2) | async-done | bytes 1048608 | tf_op jit(solution)/shard_map/all_to_all | solution.py:35
  102.0 1.1 %spread.1 = (bf16[2048,128]{1,0:T(8,128)(2,1)}, bf16[128,2048]{1,0:T(8,128)(2,1)}) custom-call(bf16[16,2,128,128]{3,2,1,0:T(8,128)(2,1)S(1)} %all-to-all-done.2.gathered), custom_call_target="tpu_custom_call" | custom-call | tf_op jit(solution)/shard_map/spread/pallas_call | solution.py:352
  (23 shorter events, 0.4 us)
Async XLA Ops:
  8.6 5.4 %collective-permute-start = (bf16[512,2048]{1,0:T(8,128)(2,1)S(1)}, bf16[512,2048]{1,0:T(8,128)(2,1)S(1)}, u32[]{:S(2)}, u32[]{:S(2)}) collective-permute-start(bf16[512,2048]{1,0:T(8,128)(2,1)S(1)} %get-tuple-element.27), channel_id=1, source_target_pairs={{0,1},{1,0},{2,3},{3,2},{4,5},{5,4},{6,7},{7,6},{8,9},{9,8},{10,11... | collective-permute-start | bytes 6291464 | tf_op jit(solution)/shard_map/ppermute | solution.py:39
  15.5 12.0 %copy-start.3 = (f32[2,128,64]{1,2,0:T(8,128)S(1)}, f32[2,128,64]{1,2,0:T(8,128)}, u32[]{:S(2)}) copy-start(f32[2,128,64]{1,2,0:T(8,128)} %param.16) | copy-start | bytes 196612
  15.5 12.0 %copy-start.4 = (f32[2,128,64]{1,2,0:T(8,128)S(1)}, f32[2,128,64]{1,2,0:T(8,128)}, u32[]{:S(2)}) copy-start(f32[2,128,64]{1,2,0:T(8,128)} %param.17) | copy-start | bytes 196612
  15.5 51.4 %copy-start = (bf16[2,1024,512]{2,1,0:T(8,128)(2,1)S(1)}, bf16[2,1024,512]{2,1,0:T(8,128)(2,1)}, u32[]{:S(2)}) copy-start(bf16[2,1024,512]{2,1,0:T(8,128)(2,1)} %bases.3) | copy-start | bytes 6291460
  15.5 42.0 %all-to-all-start = ((bf16[64,128,128]{2,1,0:T(8,128)(2,1)}), bf16[64,128,128]{2,1,0:T(8,128)(2,1)}, u32[]{:S(2)}, u32[]{:S(2)}) async-start(bf16[64,128,128]{2,1,0:T(8,128)(2,1)} %combine.1), calls=%async_computation | async-start | bytes 4194304 | tf_op jit(solution)/shard_map/all_to_all | solution.py:35
  27.5 51.6 %copy-start.1 = (f32[128,128]{1,0:T(8,128)S(1)}, f32[128,128]{1,0:T(8,128)}, u32[]{:S(2)}) copy-start(f32[128,128]{1,0:T(8,128)} %key_weight.3) | copy-start | bytes 196612
  27.5 51.6 %copy-start.2 = (f32[128,128]{1,0:T(8,128)S(1)}, f32[128,128]{1,0:T(8,128)}, u32[]{:S(2)}) copy-start(f32[128,128]{1,0:T(8,128)} %out_weight.3) | copy-start | bytes 196612
  27.6 31.9 %collective-permute-start.1 = (f32[2,64,128]{2,1,0:T(8,128)S(1)}, f32[2,64,128]{2,1,0:T(8,128)S(1)}, u32[]{:S(2)}, u32[]{:S(2)}) collective-permute-start(f32[2,64,128]{2,1,0:T(8,128)S(1)} %pad_maximum_fusion.1), channel_id=1, source_target_pairs={{0,1},{1,0},{2,3},{3,2},{4,5},{5,4},{6,7},{7,6},{8,9},{9,8},{10,11... | collective-permute-start | bytes 196616 | tf_op jit(solution)/shard_map/ppermute | solution.py:39
  59.6 5.6 %collective-permute-start.2 = (f32[128,128]{1,0:T(8,128)S(1)}, f32[128,128]{1,0:T(8,128)S(1)}, u32[]{:S(2)}, u32[]{:S(2)}) collective-permute-start(f32[128,128]{1,0:T(8,128)S(1)} %get-tuple-element.28.refs_0_), channel_id=1, source_target_pairs={{0,2},{2,4},{4,6},{6,0},{1,3},{3,5},{5,7},{7,1},{8,10},{10,12},{12... | collective-permute-start | bytes 196616 | tf_op jit(solution)/shard_map/ppermute | solution.py:395
  60.2 5.8 %collective-permute-start.3 = (f32[128,128]{1,0:T(8,128)S(1)}, f32[128,128]{1,0:T(8,128)S(1)}, u32[]{:S(2)}, u32[]{:S(2)}) collective-permute-start(f32[128,128]{1,0:T(8,128)S(1)} %get-tuple-element.28.refs_0_), channel_id=1, source_target_pairs={{0,4},{2,6},{4,0},{6,2},{1,5},{3,7},{5,1},{7,3},{8,12},{10,14},{12... | collective-permute-start | bytes 196616 | tf_op jit(solution)/shard_map/ppermute | solution.py:395
  62.7 4.3 %collective-permute-start.4 = (f32[128,128]{1,0:T(8,128)S(1)}, f32[128,128]{1,0:T(8,128)S(1)}, u32[]{:S(2)}, u32[]{:S(2)}) collective-permute-start(f32[128,128]{1,0:T(8,128)S(1)} %get-tuple-element.28.refs_0_), channel_id=1, source_target_pairs={{0,6},{2,0},{4,2},{6,4},{1,7},{3,1},{5,3},{7,5},{8,14},{10,8},{12,... | collective-permute-start | bytes 196616 | tf_op jit(solution)/shard_map/ppermute | solution.py:395
  68.0 11.0 %collective-permute-start.5 = (f32[128,128]{1,0:T(8,128)S(1)}, f32[128,128]{1,0:T(8,128)S(1)}, u32[]{:S(2)}, u32[]{:S(2)}) collective-permute-start(f32[128,128]{1,0:T(8,128)S(1)} %get-tuple-element.31), channel_id=1, source_target_pairs={{0,1},{1,0},{2,3},{3,2},{4,5},{5,4},{6,7},{7,6},{8,9},{9,8},{10,11... | collective-permute-start | bytes 196616 | tf_op jit(solution)/shard_map/ppermute | solution.py:39
  80.3 21.7 %all-to-all-start.2 = ((bf16[16,2,128,128]{3,2,1,0:T(8,128)(2,1)}), bf16[16,2,128,128]{3,2,1,0:T(8,128)(2,1)S(1)}, u32[]{:S(2)}, u32[]{:S(2)}) async-start(bf16[16,2,128,128]{3,2,1,0:T(8,128)(2,1)} %shard_map.153), calls=%async_computation.2 | async-start | bytes 2097152 | tf_op jit(solution)/shard_map/all_to_all | solution.py:35
  84.0 1.3 %collective-permute-start.6 = (f32[2,64,128]{2,1,0:T(8,128)S(1)}, f32[2,64,128]{2,1,0:T(8,128)S(1)}, u32[]{:S(2)}, u32[]{:S(2)}) collective-permute-start(f32[2,64,128]{2,1,0:T(8,128)S(1)} %broadcast_select_fusion.2), channel_id=1, source_target_pairs={{0,1},{1,0},{2,3},{3,2},{4,5},{5,4},{6,7},{7,6},{8,9},{9,8},{10,11... | collective-permute-start | bytes 196616 | tf_op jit(solution)/shard_map/ppermute | solution.py:39
where the time goes:
time: 104 us; the launch traced here: 103 us
  waiting for transfers between devices  47.9 us (46%)
  starting transfers between devices  21 us (20%)
  Pallas kernels  19.1 us (18%)
  blocking collectives  11 us (11%)
  other arithmetic  3.29 us (3%)
    all_to_all x2, waiting for transfers between devices, exchanged(): return lax.all_to_all(tiles, axes, split_axis=0, concat_axis=0, tiled=True)  44.2 us
    all_to_all x2, starting transfers between devices, exchanged(): return lax.all_to_all(tiles, axes, split_axis=0, concat_axis=0, tiled=True)  15.6 us
    all_to_all x1, blocking collectives, exchanged(): return lax.all_to_all(tiles, axes, split_axis=0, concat_axis=0, tiled=True)  11 us
    pallas_call x1, Pallas kernels, both_low(): pl.pallas_call(partner_kernel, out_shape=(pltpu.VMEM((rank, height), narr...  7.99 us
    pallas_call x1, Pallas kernels, both_low(): pl.pallas_call(own_kernel, out_shape=pltpu.VMEM((rank, height), wide), in...  5.33 us
    ppermute x3, starting transfers between devices, body(): lax.ppermute(direction, 'tp_0', [(i, (i + s) % n_x) for i in range(n_x)])  4.84 us
    ppermute x3, waiting for transfers between devices, body(): lax.ppermute(direction, 'tp_0', [(i, (i + s) % n_x) for i in range(n_x)])  2.44 us
  transfers between devices with their start and end apart: 9, of which 6 were waited for; matrix products, arithmetic and copies ran while one was open for 3% of the time, Pallas kernels for 6%

commit v1 on v0

--- a/solution.py
+++ b/solution.py
@@ -13,7 +13,6 @@
 FS = ("fs_0", "fs_1")
 TP = ("tp_0", "tp_1")
 CHIPS = ("fs_0", "tp_0", "fs_1")
-ROWS_AND_CORE = ("tp_1", "fs_0", "fs_1")
 FS_TP = ("fs_0", "fs_1", "tp_0", "tp_1")
 SWAP = [(0, 1), (1, 0)]
 LANES = 128
@@ -248,29 +247,57 @@
     )(core, low, firsts, seconds, got)
 
 
-def project_kernel(where, bases, *refs):
-    *directions, own, other, row, base, sem = refs
+def fetch_kernel(where, bases, base, sem):
+    cols = base.shape[0]
+    at = pl.ds(pl.multiple_of(where[1] * cols, cols), cols)
+    load = pltpu.make_async_copy(bases.at[where[0], at], base, sem)
+    load.start()
+    load.wait()
+
+
+def own_base(where, bases, cols):
+    return pl.pallas_call(
+        fetch_kernel,
+        out_shape=pltpu.VMEM((cols, bases.shape[2]), narrow),
+        in_specs=[in_smem, in_hbm],
+        out_specs=in_vmem,
+        scratch_shapes=[pltpu.SemaphoreType.DMA],
+        compiler_params=pltpu.CompilerParams(vmem_limit_bytes=2 * MIB),
+        name="own_base",
+    )(where, pltpu.with_memory_space_constraint(bases, pltpu.HBM))
+
+
+def squares_kernel(*refs):
+    *directions, row = refs
+    total = jnp.zeros((1, LANES), wide)
+    for part in directions:
+        value = part[...]
+        total = total + jnp.sum(value * value, axis=0, keepdims=True)
+    row[...] = jnp.broadcast_to(jnp.sum(total, axis=1, keepdims=True), row.shape)
+
+
+def squares_of(directions):
+    return pl.pallas_call(
+        squares_kernel,
+        out_shape=pltpu.VMEM((8, LANES), wide),
+        in_specs=[in_vmem] * len(directions),
+        out_specs=in_vmem,
+        compiler_params=pltpu.CompilerParams(vmem_limit_bytes=2 * MIB),
+        name="squares",
+    )(*directions)
+
+
+def project_kernel(where, base, *refs):
+    *directions, own, other = refs
     core, chip_x = (where[0], where[1])
     cols = own.shape[0]
     n_x = len(directions)
-    at = pl.ds(pl.multiple_of(chip_x * 2 * cols, 2 * cols), 2 * cols)
-    load = pltpu.make_async_copy(bases.at[core, at], base, sem)
-    load.start()
-    square = jnp.zeros((1, LANES), wide)
-    parts = []
+    total = jnp.zeros((2 * cols, own.shape[1]), wide)
     for x in range(n_x):
         part = directions[0][...]
         back = lax.rem(chip_x - x + n_x, n_x)
         for s in range(1, n_x):
             part = jnp.where(back == s, directions[s][...], part)
-        square = square + jnp.sum(part * part, axis=0, keepdims=True)
-        parts.append(part)
-    square = jnp.sum(square, axis=1, keepdims=True)
-    lanes = lax.broadcasted_iota(jnp.int32, (1, LANES), 1)
-    row[...] = jnp.broadcast_to(jnp.where(lanes == core, square, 0.0)[None], row.shape)
-    load.wait()
-    total = jnp.zeros((2 * cols, parts[0].shape[1]), wide)
-    for x, part in enumerate(parts):
         width, n = part.shape
         high = part.astype(narrow)
         rest = part - high.astype(wide)
@@ -286,45 +313,52 @@
     other[...] = jnp.where(core == 0, right, left)
 
 
-def project(where, bases, directions, cols, peers):
+def project(where, base, directions, cols):
     out = pltpu.VMEM((cols, directions[0].shape[1]), wide)
     return pl.pallas_call(
         project_kernel,
-        out_shape=(out, out, jax.ShapeDtypeStruct((peers, 1, LANES), wide)),
-        in_specs=[in_smem, in_hbm] + [in_vmem] * len(directions),
-        out_specs=(in_vmem,) * 3,
-        scratch_shapes=[
-            pltpu.VMEM((2 * cols, bases.shape[2]), narrow),
-            pltpu.SemaphoreType.DMA,
-        ],
+        out_shape=(out, out),
+        in_specs=[in_smem] + [in_vmem] * (1 + len(directions)),
+        out_specs=(in_vmem,) * 2,
         compiler_params=pltpu.CompilerParams(vmem_limit_bytes=6 * MIB),
         name="project",
-    )(where, bases, *directions)
-
-
-def steps_of(core, sums, own, came, key_weight, out_weight):
-    total = jnp.sum(sums[...], axis=0)
-    scales = lax.rsqrt(total / (D * RANK) + 1.0)
-    lanes = lax.broadcasted_iota(jnp.int32, scales.shape, 1)
-    key_scale = jnp.sum(jnp.where(lanes == 0, scales, 0.0), axis=1, keepdims=True)
-    out_scale = jnp.sum(jnp.where(lanes == 1, scales, 0.0), axis=1, keepdims=True)
+    )(where, base, *directions)
+
+
+def from_others(array, axis):
+    n = lax.axis_size(axis)
+    return [
+        lax.ppermute(array, axis, [(i, (i + s) % n) for i in range(n)]) for s in range(1, n)
+    ]
+
+
+def summed(array, axis):
+    return functools.reduce(jnp.add, from_others(array, axis), array)
+
+
+def steps_of(core, squares, partner_squares, own, came, key_weight, out_weight):
+    def scale_of(total):
+        return lax.rsqrt(total[0:1, 0:1] / (D * RANK) + 1.0)
+
     zero = core[0] == 0
-    key_step = jnp.where(zero, own[...], came[...]).T * key_scale
-    out_step = jnp.where(zero, came[...], own[...]) * out_scale
+    here, there = (own[...] * scale_of(squares), came[...] * scale_of(partner_squares))
+    key_step = jnp.where(zero, here, there).T
+    out_step = jnp.where(zero, there, here)
     key_new = key_weight[...] - learn_rate * key_step
     out_new = out_weight[...] - learn_rate * out_step
     return (key_new, out_new, key_step, out_step)
 
 
-def copies_kernel(core, sums, own, came, key_weight, out_weight, copies):
-    key_new, out_new, _, _ = steps_of(core, sums, own, came, key_weight, out_weight)
+def copies_kernel(*refs):
+    *ins, copies = refs
+    key_new, out_new, _, _ = steps_of(*ins)
     copies[...] = jnp.broadcast_to(
         jnp.stack((key_new.astype(narrow), out_new.astype(narrow)))[None], copies.shape
     )
 
 
-def steps_kernel(core, sums, own, came, key_weight, out_weight, *outs):
-    for out, value in zip(outs, steps_of(core, sums, own, came, key_weight, out_weight)):
+def steps_kernel(*refs):
+    for out, value in zip(refs[-4:], steps_of(*refs[:-4])):
         out[...] = value
 
 
@@ -332,7 +366,7 @@
     return pl.pallas_call(
         kernel,
         out_shape=outs,
-        in_specs=[in_smem] + [in_vmem] * 5,
+        in_specs=[in_smem] + [in_vmem] * 6,
         out_specs=jax.tree.map(lambda _: in_vmem, outs),
         compiler_params=pltpu.CompilerParams(vmem_limit_bytes=6 * MIB),
     )(*args)
@@ -391,17 +425,16 @@
     )
     first, second, direction = new_moments(this, low, firsts, seconds, got)
 
-    directions = [direction] + [
-        lax.ppermute(direction, "tp_0", [(i, (i + s) % n_x) for i in range(n_x)])
-        for s in range(1, n_x)
-    ]
-    own, other, row = project(
-        jnp.stack((core, chip_x)), bases, directions, cols, lax.axis_size(ROWS_AND_CORE)
-    )
-    sums = exchanged(row, ROWS_AND_CORE)
+    where = jnp.stack((core, chip_x))
+    base = own_base(where, bases, 2 * cols)
+    directions = [direction] + from_others(direction, "tp_0")
+    squares = summed(squares_of(directions), "fs_0")
+    own, other = project(where, base, directions, cols)
+    squares = summed(squares, "fs_1")
     came = swapped(other)
+    partner_squares = swapped(squares)
     square = jax.ShapeDtypeStruct((rows, cols), wide)
-    args = (this, sums, own, came, key_weight, out_weight)
+    args = (this, squares, partner_squares, own, came, key_weight, out_weight)
     copies = stepped(copies_kernel, pltpu.HBM((n_z * n_y, 2, rows, cols), narrow), *args)
     gathered = exchanged(copies, ("fs_1", "fs_0"))
     key_new, out_new, key_step, out_step = stepped(steps_kernel, (square,) * 4, *args)

time: 104 us -> 107 us (1.029)
  blocking collectives: 11 us -> 0 us
  starting transfers between devices: 21 us -> 29.6 us
  waiting for transfers between devices: 47.9 us -> 53.2 us
  other arithmetic: 3.29 us -> 1.7 us
  Pallas kernels: 19.1 us -> 20.5 us
    all_to_all x1 -> x0, blocking collectives: 11 us -> none  [exchanged(): return lax.all_to_all(tiles, axes, split_axis=0, concat_axis=0, tiled=True)]
    ppermute x3 -> x9, starting transfers between devices: 4.84 us -> 11.8 us  [from_others(): lax.ppermute(array, axis, [(i, (i + s) % n) for i in range(n)])]
    ppermute x3 -> x9, waiting for transfers between devices: 2.44 us -> 6.27 us  [from_others(): lax.ppermute(array, axis, [(i, (i + s) % n) for i in range(n)])]
    all_to_all x2, starting transfers between devices: 15.6 us -> 17.2 us  [exchanged(): return lax.all_to_all(tiles, axes, split_axis=0, concat_axis=0, tiled=True)]
    reduce_sum x1, other arithmetic: 1.9 us -> 0.31 us  [body(): low = arrived.astype(wide).sum(axis=0)]
    pallas_call x3 -> x5, Pallas kernels: 3.13 us -> 4.52 us  [the longest x2 1.99 us: stepped(): pl.pallas_call(kernel, out_shape=outs, in_specs=[in_smem] + [in_vmem] * 6...]
    ppermute x4 -> x5, waiting for transfers between devices: 1.25 us -> 2.41 us  [swapped(): return lax.ppermute(array, 'tp_1', SWAP)]
  transfers between devices with their start and end apart: 9 -> 16, of which waited for: 6 -> 11; matrix products, arithmetic and copies ran while one was open for 3% -> 2% of each run, Pallas kernels for 6% -> 8%
where the time goes in v1:
time: 107 us; the launch traced here: 106 us
  waiting for transfers between devices  53.2 us (50%)
  starting transfers between devices  29.6 us (28%)
  Pallas kernels  20.5 us (19%)
  other arithmetic  1.7 us (2%)
    all_to_all x2, waiting for transfers between devices, exchanged(): return lax.all_to_all(tiles, axes, split_axis=0, concat_axis=0, tiled=True)  44.6 us
    all_to_all x2, starting transfers between devices, exchanged(): return lax.all_to_all(tiles, axes, split_axis=0, concat_axis=0, tiled=True)  17.2 us
    ppermute x9, starting transfers between devices, from_others(): lax.ppermute(array, axis, [(i, (i + s) % n) for i in range(n)])  11.8 us
    pallas_call x1, Pallas kernels, both_low(): pl.pallas_call(partner_kernel, out_shape=(pltpu.VMEM((rank, height), narr...  7.99 us
    ppermute x9, waiting for transfers between devices, from_others(): lax.ppermute(array, axis, [(i, (i + s) % n) for i in range(n)])  6.27 us
    pallas_call x1, Pallas kernels, both_low(): pl.pallas_call(own_kernel, out_shape=pltpu.VMEM((rank, height), wide), in...  5.33 us
    ppermute x5, waiting for transfers between devices, swapped(): return lax.ppermute(array, 'tp_1', SWAP)  2.41 us
  transfers between devices with their start and end apart: 16, of which 11 were waited for; matrix products, arithmetic and copies ran while one was open for 2% of the time, Pallas kernels for 8%

profile of v1, /device:TPU:0, one launch (start us, length us, event | category | flops | bytes accessed | tf_op | source)
XLA Modules:
  0.0 106.0 jit_solution(15084351283544751501)
XLA Ops:
  0.6 8.0 %partner_low.1 = (bf16[512,2048]{1,0:T(8,128)(2,1)S(1)}, bf16[768,2048]{1,0:T(8,128)(2,1)S(1)}, bf16[1536,1024]{1,0:T(8,128)(2,1)S(1)}, bf16[1024,512]{1,0:T(8,128)(2,1)S(1)}) custom-call(s32[1]{0:T(128)} %bitcast.core.refs_0_, bf16[1536,2048]{1,0:T(8,128)(2,1)} %rows0.3, bf16[1536,1024]{1,0:T(8,128)(2,1)} %cols0.1, bf16[1536,2048]{1,0:T(8,128)(2,1)} %rows1.3, ...), custom_call_target="tpu_custom_call" | custom-call | flops 4831838208 | bytes 9437184 | tf_op jit(solution)/shard_map/partner_low/pallas_call | solution.py:157
  8.7 5.3 %own_low.1.mine = f32[512,2048]{1,0:T(8,128)S(1)} custom-call(s32[1]{0:T(128)} %bitcast.core.refs_0_, bf16[1536,2048]{1,0:T(8,128)(2,1)} %rows0.3, bf16[1536,2048]{1,0:T(8,128)(2,1)} %rows1.3, bf16[768,2048]{1,0:T(8,128)(2,1)S(1)} %get-tuple-element.23.rows, bf16[1536,1024]{1,0:T(8,128)(2,1)S(1)} %get-tuple-element.24.cols, ...), custom_call_target="tpu_custom_call" | custom-call | flops 4831838208 | bytes 9437184 | tf_op jit(solution)/shard_map/own_low/pallas_call | solution.py:179
  14.1 1.5 %combine.1 = bf16[64,128,128]{2,1,0:T(8,128)(2,1)} custom-call(f32[512,2048]{1,0:T(8,128)S(1)} %own_low.1.mine, bf16[512,2048]{1,0:T(8,128)(2,1)S(1)} %collective-permute-done.partner), custom_call_target="tpu_custom_call" | custom-call | tf_op jit(solution)/shard_map/combine/pallas_call | solution.py:213
  15.6 11.7 %all-to-all-start = ((bf16[64,128,128]{2,1,0:T(8,128)(2,1)}), bf16[64,128,128]{2,1,0:T(8,128)(2,1)S(1)}, u32[]{:S(2)}, u32[]{:S(2)}) async-start(bf16[64,128,128]{2,1,0:T(8,128)(2,1)} %combine.1), calls=%async_computation | async-start | bytes 4194304 | tf_op jit(solution)/shard_map/all_to_all | solution.py:34
  27.6 29.9 %all-to-all-done = bf16[64,128,128]{2,1,0:T(8,128)(2,1)S(1)} async-done(((bf16[64,128,128]{2,1,0:T(8,128)(2,1)}), bf16[64,128,128]{2,1,0:T(8,128)(2,1)S(1)}, u32[]{:S(2)}, u32[]{:S(2)}) %all-to-all-start) | async-done | bytes 2097184 | tf_op jit(solution)/shard_map/all_to_all | solution.py:34
  58.6 2.4 %collective-permute-start.3 = (f32[128,128]{1,0:T(8,128)S(1)}, f32[128,128]{1,0:T(8,128)S(1)}, u32[]{:S(2)}, u32[]{:S(2)}) collective-permute-start(f32[128,128]{1,0:T(8,128)S(1)} %get-tuple-element.27.refs_0_), channel_id=1, source_target_pairs={{0,4},{2,6},{4,0},{6,2},{1,5},{3,7},{5,1},{7,3},{8,12},{10,14},{12... | collective-permute-start | bytes 196616 | tf_op jit(solution)/shard_map/ppermute | solution.py:331
  61.0 1.7 %collective-permute-start.4 = (f32[128,128]{1,0:T(8,128)S(1)}, f32[128,128]{1,0:T(8,128)S(1)}, u32[]{:S(2)}, u32[]{:S(2)}) collective-permute-start(f32[128,128]{1,0:T(8,128)S(1)} %get-tuple-element.27.refs_0_), channel_id=1, source_target_pairs={{0,6},{2,0},{4,2},{6,4},{1,7},{3,1},{5,3},{7,5},{8,14},{10,8},{12,... | collective-permute-start | bytes 196616 | tf_op jit(solution)/shard_map/ppermute | solution.py:331
  63.5 0.8 collective-permute-done.3.refs_2_
  64.3 0.9 collective-permute-done.4.refs_3_
  66.1 1.9 %collective-permute-start.6 = (f32[8,128]{1,0:T(8,128)S(1)}, f32[8,128]{1,0:T(8,128)S(1)}, u32[]{:S(2)}, u32[]{:S(2)}) collective-permute-start(f32[8,128]{1,0:T(8,128)S(1)} %squares.1), channel_id=1, source_target_pairs={{0,64},{32,96},{64,0},{96,32},{1,65},{33,97},{65,1},{97,33},{2,66}... | collective-permute-start | bytes 12296 | tf_op jit(solution)/shard_map/ppermute | solution.py:331
  68.0 0.9 collective-permute-start.7
  68.9 1.3 %collective-permute-done.5 = f32[8,128]{1,0:T(8,128)S(1)} collective-permute-done((f32[8,128]{1,0:T(8,128)S(1)}, f32[8,128]{1,0:T(8,128)S(1)}, u32[]{:S(2)}, u32[]{:S(2)}) %collective-permute-start.5) | collective-permute-done | bytes 4128 | tf_op jit(solution)/shard_map/ppermute | solution.py:331
  70.2 1.0 collective-permute-done.6
  72.0 1.6 %collective-permute-start.8 = (f32[8,128]{1,0:T(8,128)S(1)}, f32[8,128]{1,0:T(8,128)S(1)}, u32[]{:S(2)}, u32[]{:S(2)}) collective-permute-start(f32[8,128]{1,0:T(8,128)S(1)} %add_add_fusion.1), channel_id=1, source_target_pairs={{0,8},{8,16},{16,24},{24,0},{1,9},{9,17},{17,25},{25,1},{2,10},{10... | collective-permute-start | bytes 12296 | tf_op jit(solution)/shard_map/ppermute | solution.py:331
  73.6 1.5 %collective-permute-start.9 = (f32[8,128]{1,0:T(8,128)S(1)}, f32[8,128]{1,0:T(8,128)S(1)}, u32[]{:S(2)}, u32[]{:S(2)}) collective-permute-start(f32[8,128]{1,0:T(8,128)S(1)} %add_add_fusion.1), channel_id=1, source_target_pairs={{0,16},{8,24},{16,0},{24,8},{1,17},{9,25},{17,1},{25,9},{2,18},{10... | collective-permute-start | bytes 12296 | tf_op jit(solution)/shard_map/ppermute | solution.py:331
  75.1 1.5 %own_base.1.base = bf16[256,512]{1,0:T(8,128)(2,1)S(1)} custom-call(s32[2]{0:T(128)S(1)} %pad_add_fusion.where, bf16[2,1024,512]{2,1,0:T(8,128)(2,1)} %bases.3), custom_call_target="tpu_custom_call" | custom-call | tf_op jit(solution)/shard_map/own_base/pallas_call | solution.py:259
  76.7 0.9 project.1
  77.7 1.0 collective-permute-done.9
  78.7 1.2 %collective-permute-done.11.refs_2_ = f32[8,128]{1,0:T(8,128)S(1)} collective-permute-done((f32[8,128]{1,0:T(8,128)S(1)}, f32[8,128]{1,0:T(8,128)S(1)}, u32[]{:S(2)}, u32[]{:S(2)}) %collective-permute-start.11) | collective-permute-done | bytes 4128 | tf_op jit(solution)/shard_map/ppermute | solution.py:38
  79.9 1.2 %shard_map.153 = bf16[16,2,128,128]{3,2,1,0:T(8,128)(2,1)} custom-call(s32[1]{0:T(128)} %bitcast.core.refs_0_, f32[8,128]{1,0:T(8,128)S(1)} %add_add_fusion.refs_1_, f32[8,128]{1,0:T(8,128)S(1)} %collective-permute-done.11.refs_2_, f32[128,128]{1,0:T(8,128)S(1)} %get-tuple-element.28.refs_3_, f32[128,128]{1,0:T(8,128)S(1)} %collective-permute-done.12.refs_4_, ...), custom_call_target="tpu_custom_call" | custom-call | tf_op jit(solution)/shard_map/pallas_call | solution.py:366
  81.1 5.6 %all-to-all-start.1 = ((bf16[16,2,128,128]{3,2,1,0:T(8,128)(2,1)}), bf16[16,2,128,128]{3,2,1,0:T(8,128)(2,1)S(1)}, u32[]{:S(2)}, u32[]{:S(2)}) async-start(bf16[16,2,128,128]{3,2,1,0:T(8,128)(2,1)} %shard_map.153), calls=%async_computation.1 | async-start | bytes 2097152 | tf_op jit(solution)/shard_map/all_to_all | solution.py:34
  86.8 1.2 %collective-permute-done.13 = f32[2,64,128]{2,1,0:T(8,128)S(1)} collective-permute-done((f32[2,64,128]{2,1,0:T(8,128)S(1)}, f32[2,64,128]{2,1,0:T(8,128)S(1)}, u32[]{:S(2)}, u32[]{:S(2)}) %collective-permute-start.13) | collective-permute-done | bytes 65568 | tf_op jit(solution)/shard_map/ppermute | solution.py:38
  90.1 14.7 %all-to-all-done.1.gathered = bf16[16,2,128,128]{3,2,1,0:T(8,128)(2,1)S(1)} async-done(((bf16[16,2,128,128]{3,2,1,0:T(8,128)(2,1)}), bf16[16,2,128,128]{3,2,1,0:T(8,128)(2,1)S(1)}, u32[]{:S(2)}, u32[]{:S(2)}) %all-to-all-start.1) | async-done | bytes 1048608 | tf_op jit(solution)/shard_map/all_to_all | solution.py:34
  104.8 1.1 %spread.1 = (bf16[2048,128]{1,0:T(8,128)(2,1)}, bf16[128,2048]{1,0:T(8,128)(2,1)}) custom-call(bf16[16,2,128,128]{3,2,1,0:T(8,128)(2,1)S(1)} %all-to-all-done.1.gathered), custom_call_target="tpu_custom_call" | custom-call | tf_op jit(solution)/shard_map/spread/pallas_call | solution.py:386
  (38 shorter events, 6.2 us)
Async XLA Ops:
  8.6 5.4 %collective-permute-start = (bf16[512,2048]{1,0:T(8,128)(2,1)S(1)}, bf16[512,2048]{1,0:T(8,128)(2,1)S(1)}, u32[]{:S(2)}, u32[]{:S(2)}) collective-permute-start(bf16[512,2048]{1,0:T(8,128)(2,1)S(1)} %get-tuple-element.26), channel_id=1, source_target_pairs={{0,1},{1,0},{2,3},{3,2},{4,5},{5,4},{6,7},{7,6},{8,9},{9,8},{10,11... | collective-permute-start | bytes 6291464 | tf_op jit(solution)/shard_map/ppermute | solution.py:38
  15.6 11.7 %copy-start = (f32[2,128,64]{1,2,0:T(8,128)S(1)}, f32[2,128,64]{1,2,0:T(8,128)}, u32[]{:S(2)}) copy-start(f32[2,128,64]{1,2,0:T(8,128)} %param.16) | copy-start | bytes 196612
  15.6 11.7 %copy-start.1 = (f32[2,128,64]{1,2,0:T(8,128)S(1)}, f32[2,128,64]{1,2,0:T(8,128)}, u32[]{:S(2)}) copy-start(f32[2,128,64]{1,2,0:T(8,128)} %param.17) | copy-start | bytes 196612
  15.6 41.9 %all-to-all-start = ((bf16[64,128,128]{2,1,0:T(8,128)(2,1)}), bf16[64,128,128]{2,1,0:T(8,128)(2,1)S(1)}, u32[]{:S(2)}, u32[]{:S(2)}) async-start(bf16[64,128,128]{2,1,0:T(8,128)(2,1)} %combine.1), calls=%async_computation | async-start | bytes 4194304 | tf_op jit(solution)/shard_map/all_to_all | solution.py:34
  27.3 52.6 %copy-start.2 = (f32[128,128]{1,0:T(8,128)S(1)}, f32[128,128]{1,0:T(8,128)}, u32[]{:S(2)}) copy-start(f32[128,128]{1,0:T(8,128)} %refs_5_.3) | copy-start | bytes 196612
  27.3 52.6 %copy-start.3 = (f32[128,128]{1,0:T(8,128)S(1)}, f32[128,128]{1,0:T(8,128)}, u32[]{:S(2)}) copy-start(f32[128,128]{1,0:T(8,128)} %refs_6_.3) | copy-start | bytes 196612
  27.3 30.5 %collective-permute-start.1 = (f32[2,64,128]{2,1,0:T(8,128)S(1)}, f32[2,64,128]{2,1,0:T(8,128)S(1)}, u32[]{:S(2)}, u32[]{:S(2)}) collective-permute-start(f32[2,64,128]{2,1,0:T(8,128)S(1)} %pad_maximum_fusion.1), channel_id=1, source_target_pairs={{0,1},{1,0},{2,3},{3,2},{4,5},{5,4},{6,7},{7,6},{8,9},{9,8},{10,11... | collective-permute-start | bytes 196616 | tf_op jit(solution)/shard_map/ppermute | solution.py:38
  57.9 5.6 %collective-permute-start.2 = (f32[128,128]{1,0:T(8,128)S(1)}, f32[128,128]{1,0:T(8,128)S(1)}, u32[]{:S(2)}, u32[]{:S(2)}) collective-permute-start(f32[128,128]{1,0:T(8,128)S(1)} %get-tuple-element.27.refs_0_), channel_id=1, source_target_pairs={{0,2},{2,4},{4,6},{6,0},{1,3},{3,5},{5,7},{7,1},{8,10},{10,12},{12... | collective-permute-start | bytes 196616 | tf_op jit(solution)/shard_map/ppermute | solution.py:331
  58.6 5.8 %collective-permute-start.3 = (f32[128,128]{1,0:T(8,128)S(1)}, f32[128,128]{1,0:T(8,128)S(1)}, u32[]{:S(2)}, u32[]{:S(2)}) collective-permute-start(f32[128,128]{1,0:T(8,128)S(1)} %get-tuple-element.27.refs_0_), channel_id=1, source_target_pairs={{0,4},{2,6},{4,0},{6,2},{1,5},{3,7},{5,1},{7,3},{8,12},{10,14},{12... | collective-permute-start | bytes 196616 | tf_op jit(solution)/shard_map/ppermute | solution.py:331
  61.0 4.3 %collective-permute-start.4 = (f32[128,128]{1,0:T(8,128)S(1)}, f32[128,128]{1,0:T(8,128)S(1)}, u32[]{:S(2)}, u32[]{:S(2)}) collective-permute-start(f32[128,128]{1,0:T(8,128)S(1)} %get-tuple-element.27.refs_0_), channel_id=1, source_target_pairs={{0,6},{2,0},{4,2},{6,4},{1,7},{3,1},{5,3},{7,5},{8,14},{10,8},{12,... | collective-permute-start | bytes 196616 | tf_op jit(solution)/shard_map/ppermute | solution.py:331
  65.4 4.8 %collective-permute-start.5 = (f32[8,128]{1,0:T(8,128)S(1)}, f32[8,128]{1,0:T(8,128)S(1)}, u32[]{:S(2)}, u32[]{:S(2)}) collective-permute-start(f32[8,128]{1,0:T(8,128)S(1)} %squares.1), channel_id=1, source_target_pairs={{0,32},{32,64},{64,96},{96,0},{1,33},{33,65},{65,97},{97,1},{2,34}... | collective-permute-start | bytes 12296 | tf_op jit(solution)/shard_map/ppermute | solution.py:331
  66.1 5.1 %collective-permute-start.6 = (f32[8,128]{1,0:T(8,128)S(1)}, f32[8,128]{1,0:T(8,128)S(1)}, u32[]{:S(2)}, u32[]{:S(2)}) collective-permute-start(f32[8,128]{1,0:T(8,128)S(1)} %squares.1), channel_id=1, source_target_pairs={{0,64},{32,96},{64,0},{96,32},{1,65},{33,97},{65,1},{97,33},{2,66}... | collective-permute-start | bytes 12296 | tf_op jit(solution)/shard_map/ppermute | solution.py:331
  68.0 3.6 %collective-permute-start.7 = (f32[8,128]{1,0:T(8,128)S(1)}, f32[8,128]{1,0:T(8,128)S(1)}, u32[]{:S(2)}, u32[]{:S(2)}) collective-permute-start(f32[8,128]{1,0:T(8,128)S(1)} %squares.1), channel_id=1, source_target_pairs={{0,96},{32,0},{64,32},{96,64},{1,97},{33,1},{65,33},{97,65},{2,98}... | collective-permute-start | bytes 12296 | tf_op jit(solution)/shard_map/ppermute | solution.py:331
  71.6 6.1 %collective-permute-start.10 = (f32[8,128]{1,0:T(8,128)S(1)}, f32[8,128]{1,0:T(8,128)S(1)}, u32[]{:S(2)}, u32[]{:S(2)}) collective-permute-start(f32[8,128]{1,0:T(8,128)S(1)} %add_add_fusion.1), channel_id=1, source_target_pairs={{0,24},{8,0},{16,8},{24,16},{1,25},{9,1},{17,9},{25,17},{2,26},{10... | collective-permute-start | bytes 12296 | tf_op jit(solution)/shard_map/ppermute | solution.py:331
  72.0 5.7 %collective-permute-start.8 = (f32[8,128]{1,0:T(8,128)S(1)}, f32[8,128]{1,0:T(8,128)S(1)}, u32[]{:S(2)}, u32[]{:S(2)}) collective-permute-start(f32[8,128]{1,0:T(8,128)S(1)} %add_add_fusion.1), channel_id=1, source_target_pairs={{0,8},{8,16},{16,24},{24,0},{1,9},{9,17},{17,25},{25,1},{2,10},{10... | collective-permute-start | bytes 12296 | tf_op jit(solution)/shard_map/ppermute | solution.py:331
  73.6 5.1 %collective-permute-start.9 = (f32[8,128]{1,0:T(8,128)S(1)}, f32[8,128]{1,0:T(8,128)S(1)}, u32[]{:S(2)}, u32[]{:S(2)}) collective-permute-start(f32[8,128]{1,0:T(8,128)S(1)} %add_add_fusion.1), channel_id=1, source_target_pairs={{0,16},{8,24},{16,0},{24,8},{1,17},{9,25},{17,1},{25,9},{2,18},{10... | collective-permute-start | bytes 12296 | tf_op jit(solution)/shard_map/ppermute | solution.py:331
  77.6 2.3 %collective-permute-start.12 = (f32[128,128]{1,0:T(8,128)S(1)}, f32[128,128]{1,0:T(8,128)S(1)}, u32[]{:S(2)}, u32[]{:S(2)}) collective-permute-start(f32[128,128]{1,0:T(8,128)S(1)} %get-tuple-element.29), channel_id=1, source_target_pairs={{0,1},{1,0},{2,3},{3,2},{4,5},{5,4},{6,7},{7,6},{8,9},{9,8},{10,11... | collective-permute-start | bytes 196616 | tf_op jit(solution)/shard_map/ppermute | solution.py:38
  78.7 1.2 %collective-permute-start.11 = (f32[8,128]{1,0:T(8,128)S(1)}, f32[8,128]{1,0:T(8,128)S(1)}, u32[]{:S(2)}, u32[]{:S(2)}) collective-permute-start(f32[8,128]{1,0:T(8,128)S(1)} %add_add_fusion.refs_1_), channel_id=1, source_target_pairs={{0,1},{1,0},{2,3},{3,2},{4,5},{5,4},{6,7},{7,6},{8,9},{9,8},{10,11... | collective-permute-start | bytes 12296 | tf_op jit(solution)/shard_map/ppermute | solution.py:38
  81.1 23.7 %all-to-all-start.1 = ((bf16[16,2,128,128]{3,2,1,0:T(8,128)(2,1)}), bf16[16,2,128,128]{3,2,1,0:T(8,128)(2,1)S(1)}, u32[]{:S(2)}, u32[]{:S(2)}) async-start(bf16[16,2,128,128]{3,2,1,0:T(8,128)(2,1)} %shard_map.153), calls=%async_computation.1 | async-start | bytes 2097152 | tf_op jit(solution)/shard_map/all_to_all | solution.py:34
  86.7 1.3 %collective-permute-start.13 = (f32[2,64,128]{2,1,0:T(8,128)S(1)}, f32[2,64,128]{2,1,0:T(8,128)S(1)}, u32[]{:S(2)}, u32[]{:S(2)}) collective-permute-start(f32[2,64,128]{2,1,0:T(8,128)S(1)} %broadcast_select_fusion.2), channel_id=1, source_target_pairs={{0,1},{1,0},{2,3},{3,2},{4,5},{5,4},{6,7},{7,6},{8,9},{9,8},{10,11... | collective-permute-start | bytes 196616 | tf_op jit(solution)/shard_map/ppermute | solution.py:38

commit v2 on v1

--- a/solution.py
+++ b/solution.py
@@ -16,6 +16,9 @@
 FS_TP = ("fs_0", "fs_1", "tp_0", "tp_1")
 SWAP = [(0, 1), (1, 0)]
 LANES = 128
+CHIPS_TURN = 42
+SQUARES_TURN = 0
+GATHER_TURN = 10
 MIB = 2**20
 
 
@@ -30,8 +33,15 @@
 in_vmem = pl.BlockSpec(memory_space=pltpu.VMEM)
 
 
-def exchanged(tiles, axes):
-    return lax.all_to_all(tiles, axes, split_axis=0, concat_axis=0, tiled=True)
+def turned(n, turn):
+    return [(i + turn) % n for i in range(n)]
+
+
+def exchanged(tiles, axes, turn=0):
+    groups = [turned(lax.axis_size(axes), turn)] if turn else None
+    return lax.all_to_all(
+        tiles, axes, split_axis=0, concat_axis=0, axis_index_groups=groups, tiled=True
+    )
 
 
 def swapped(array):
@@ -195,17 +205,17 @@
 
 def combine_kernel(mine, partner, out, tiles, sems, *, n_x, n_y):
     count = out.shape[0] // sems.shape[0]
-    for z in range(sems.shape[0]):
-        for x in range(n_x):
-            for y in range(n_y):
-                ranks, rows = (pl.ds(x * LANES, LANES), pl.ds((z * n_y + y) * LANES, LANES))
-                total = mine[ranks, rows] + partner[ranks, rows].astype(wide)
-                tiles[(z * n_x + x) * n_y + y] = total.astype(narrow)
-        at = pl.ds(z * count, count)
-        pltpu.make_async_copy(tiles.at[at], out.at[at], sems.at[z]).start()
-    for z in range(sems.shape[0]):
-        at = pl.ds(z * count, count)
-        pltpu.make_async_copy(tiles.at[at], out.at[at], sems.at[z]).wait()
+    for j, chip in enumerate(turned(out.shape[0], CHIPS_TURN)):
+        z, x, y = (chip // (n_x * n_y), chip // n_y % n_x, chip % n_y)
+        ranks, rows = (pl.ds(x * LANES, LANES), pl.ds((z * n_y + y) * LANES, LANES))
+        total = mine[ranks, rows] + partner[ranks, rows].astype(wide)
+        tiles[j] = total.astype(narrow)
+        if (j + 1) % count == 0:
+            at = pl.ds(j + 1 - count, count)
+            pltpu.make_async_copy(tiles.at[at], out.at[at], sems.at[j // count]).start()
+    for k in range(sems.shape[0]):
+        at = pl.ds(k * count, count)
+        pltpu.make_async_copy(tiles.at[at], out.at[at], sems.at[k]).wait()
 
 
 def combine(mine, partner, n_z, n_y, n_x):
@@ -215,13 +225,13 @@
         out_shape=pltpu.HBM(shape, narrow),
         in_specs=[in_vmem] * 2,
         out_specs=in_hbm,
-        scratch_shapes=[pltpu.VMEM(shape, narrow), pltpu.SemaphoreType.DMA((n_z,))],
+        scratch_shapes=[pltpu.VMEM(shape, narrow), pltpu.SemaphoreType.DMA((4,))],
         compiler_params=pltpu.CompilerParams(vmem_limit_bytes=8 * MIB),
         name="combine",
     )(mine, partner)
 
 
-def moments_kernel(core, low, firsts, seconds, got, first, second, direction):
+def moments_kernel(core, low, firsts, seconds, got, first, second, direction, row):
     zero = core[0] == 0
 
     def joined(old, came):
@@ -231,17 +241,22 @@
     sums = low[...]
     first_new = first_decay * joined(firsts, got[0]) + (1.0 - first_decay) * sums
     second_new = second_decay * joined(seconds, got[1]) + (1.0 - second_decay) * sums * sums
+    ratio = first_new / jnp.sqrt(second_new)
     first[...] = first_new
     second[...] = second_new
-    direction[...] = first_new / jnp.sqrt(second_new)
-
-
-def new_moments(core, low, firsts, seconds, got):
+    direction[...] = ratio
+    square = jnp.sum(jnp.sum(ratio * ratio, axis=0, keepdims=True), axis=1, keepdims=True)
+    lanes = lax.broadcasted_iota(jnp.int32, (1, LANES), 1)
+    row[...] = jnp.broadcast_to(jnp.where(lanes == core[0], square, 0.0)[None], row.shape)
+
+
+def new_moments(core, low, firsts, seconds, got, everyone):
     return pl.pallas_call(
         moments_kernel,
-        out_shape=(pltpu.VMEM(low.shape, wide),) * 3,
+        out_shape=(pltpu.VMEM(low.shape, wide),) * 3
+        + (pltpu.HBM((everyone, 1, LANES), wide),),
         in_specs=[in_smem] + [in_vmem] * 4,
-        out_specs=(in_vmem,) * 3,
+        out_specs=(in_vmem,) * 4,
         compiler_params=pltpu.CompilerParams(vmem_limit_bytes=4 * MIB),
         name="moments",
     )(core, low, firsts, seconds, got)
@@ -265,26 +280,6 @@
         compiler_params=pltpu.CompilerParams(vmem_limit_bytes=2 * MIB),
         name="own_base",
     )(where, pltpu.with_memory_space_constraint(bases, pltpu.HBM))
-
-
-def squares_kernel(*refs):
-    *directions, row = refs
-    total = jnp.zeros((1, LANES), wide)
-    for part in directions:
-        value = part[...]
-        total = total + jnp.sum(value * value, axis=0, keepdims=True)
-    row[...] = jnp.broadcast_to(jnp.sum(total, axis=1, keepdims=True), row.shape)
-
-
-def squares_of(directions):
-    return pl.pallas_call(
-        squares_kernel,
-        out_shape=pltpu.VMEM((8, LANES), wide),
-        in_specs=[in_vmem] * len(directions),
-        out_specs=in_vmem,
-        compiler_params=pltpu.CompilerParams(vmem_limit_bytes=2 * MIB),
-        name="squares",
-    )(*directions)
 
 
 def project_kernel(where, base, *refs):
@@ -332,18 +327,11 @@
     ]
 
 
-def summed(array, axis):
-    return functools.reduce(jnp.add, from_others(array, axis), array)
-
-
-def steps_of(core, squares, partner_squares, own, came, key_weight, out_weight):
-    def scale_of(total):
-        return lax.rsqrt(total[0:1, 0:1] / (D * RANK) + 1.0)
-
+def steps_of(core, sums, own, came, key_weight, out_weight):
+    scales = lax.rsqrt(jnp.sum(sums[...], axis=0) / (D * RANK) + 1.0)
     zero = core[0] == 0
-    here, there = (own[...] * scale_of(squares), came[...] * scale_of(partner_squares))
-    key_step = jnp.where(zero, here, there).T
-    out_step = jnp.where(zero, there, here)
+    key_step = jnp.where(zero, own[...], came[...]).T * scales[:, 0:1]
+    out_step = jnp.where(zero, came[...], own[...]) * scales[:, 1:2]
     key_new = key_weight[...] - learn_rate * key_step
     out_new = out_weight[...] - learn_rate * out_step
     return (key_new, out_new, key_step, out_step)
@@ -366,7 +354,7 @@
     return pl.pallas_call(
         kernel,
         out_shape=outs,
-        in_specs=[in_smem] + [in_vmem] * 6,
+        in_specs=[in_smem] + [in_vmem] * 5,
         out_specs=jax.tree.map(lambda _: in_vmem, outs),
         compiler_params=pltpu.CompilerParams(vmem_limit_bytes=6 * MIB),
     )(*args)
@@ -374,11 +362,11 @@
 
 def spread_kernel(gathered, key_copy, out_copy, *, n_y):
     n_z = gathered.shape[0] // n_y
-    for y in range(n_y):
-        for z in range(n_z):
-            at = pl.ds((z * n_y + y) * LANES, LANES)
-            key_copy[at, :] = gathered[y * n_z + z, 0]
-            out_copy[:, at] = gathered[y * n_z + z, 1]
+    for i, source in enumerate(turned(gathered.shape[0], GATHER_TURN)):
+        y, z = divmod(source, n_z)
+        at = pl.ds((z * n_y + y) * LANES, LANES)
+        key_copy[at, :] = gathered[i, 0]
+        out_copy[:, at] = gathered[i, 1]
 
 
 def spread(gathered, n_y):
@@ -415,7 +403,7 @@
     this = core.reshape(1)
 
     mine, from_partner = both_low(this, saved_input, key_cot, out_cot, mixed_out, bases)
-    arrived = exchanged(combine(mine, from_partner, n_z, n_y, n_x), CHIPS)
+    arrived = exchanged(combine(mine, from_partner, n_z, n_y, n_x), CHIPS, CHIPS_TURN)
     low = arrived.astype(wide).sum(axis=0)
 
     firsts = first_moment.transpose(0, 2, 1)
@@ -423,20 +411,20 @@
     got = swapped(
         jnp.stack((pick(core, firsts[1], firsts[0]), pick(core, seconds[1], seconds[0])))
     )
-    first, second, direction = new_moments(this, low, firsts, seconds, got)
+    first, second, direction, row = new_moments(
+        this, low, firsts, seconds, got, lax.axis_size(FS_TP)
+    )
 
     where = jnp.stack((core, chip_x))
     base = own_base(where, bases, 2 * cols)
     directions = [direction] + from_others(direction, "tp_0")
-    squares = summed(squares_of(directions), "fs_0")
+    sums = exchanged(row, FS_TP, SQUARES_TURN)
     own, other = project(where, base, directions, cols)
-    squares = summed(squares, "fs_1")
     came = swapped(other)
-    partner_squares = swapped(squares)
     square = jax.ShapeDtypeStruct((rows, cols), wide)
-    args = (this, squares, partner_squares, own, came, key_weight, out_weight)
+    args = (this, sums, own, came, key_weight, out_weight)
     copies = stepped(copies_kernel, pltpu.HBM((n_z * n_y, 2, rows, cols), narrow), *args)
-    gathered = exchanged(copies, ("fs_1", "fs_0"))
+    gathered = exchanged(copies, ("fs_1", "fs_0"), GATHER_TURN)
     key_new, out_new, key_step, out_step = stepped(steps_kernel, (square,) * 4, *args)
     key_copy, out_copy = spread(gathered, n_y)
 

time: 107 us -> 105 us (0.981)
  blocking collectives: 0 us -> 18.2 us
  waiting for transfers between devices: 53.2 us -> 36.9 us
  starting transfers between devices: 29.6 us -> 25.4 us
    all_to_all x0 -> x1, blocking collectives: none -> 18.2 us  [exchanged(): lax.all_to_all(tiles, axes, split_axis=0, concat_axis=0, axis_index_group...]
    all_to_all x2, waiting for transfers between devices: 44.6 us -> 34 us  [exchanged(): lax.all_to_all(tiles, axes, split_axis=0, concat_axis=0, axis_index_group...]
    ppermute x9 -> x3, starting transfers between devices: 11.8 us -> 3.8 us  [from_others(): lax.ppermute(array, axis, [(i, (i + s) % n) for i in range(n)])]
    ppermute x9 -> x3, waiting for transfers between devices: 6.27 us -> 1.67 us  [from_others(): lax.ppermute(array, axis, [(i, (i + s) % n) for i in range(n)])]
    all_to_all x2, starting transfers between devices: 17.2 us -> 21.3 us  [exchanged(): lax.all_to_all(tiles, axes, split_axis=0, concat_axis=0, axis_index_group...]
    ppermute x5 -> x4, waiting for transfers between devices: 2.41 us -> 1.25 us  [swapped(): return lax.ppermute(array, 'tp_1', SWAP)]
    pallas_call x3 -> x2, Pallas kernels: 2.1 us -> 2.26 us  [stepped(): pl.pallas_call(kernel, out_shape=outs, in_specs=[in_smem] + [in_vmem] * 5...]
  transfers between devices with their start and end apart: 16 -> 9, of which waited for: 11 -> 5; matrix products, arithmetic and copies ran while one was open for 2% -> 2% of each run, Pallas kernels for 8% -> 7%
where the time goes in v2:
time: 105 us; the launch traced here: 104 us
  waiting for transfers between devices  36.9 us (35%)
  starting transfers between devices  25.4 us (24%)
  Pallas kernels  21.4 us (20%)
  blocking collectives  18.2 us (17%)
  other arithmetic  1.69 us (2%)
    all_to_all x2, waiting for transfers between devices, exchanged(): lax.all_to_all(tiles, axes, split_axis=0, concat_axis=0, axis_index_group...  34 us
    all_to_all x2, starting transfers between devices, exchanged(): lax.all_to_all(tiles, axes, split_axis=0, concat_axis=0, axis_index_group...  21.3 us
    all_to_all x1, blocking collectives, exchanged(): lax.all_to_all(tiles, axes, split_axis=0, concat_axis=0, axis_index_group...  18.2 us
    pallas_call x1, Pallas kernels, both_low(): pl.pallas_call(partner_kernel, out_shape=(pltpu.VMEM((rank, height), narr...  7.99 us
    pallas_call x1, Pallas kernels, both_low(): pl.pallas_call(own_kernel, out_shape=pltpu.VMEM((rank, height), wide), in...  5.33 us
    ppermute x3, starting transfers between devices, from_others(): lax.ppermute(array, axis, [(i, (i + s) % n) for i in range(n)])  3.8 us
    pallas_call x2, Pallas kernels, stepped(): pl.pallas_call(kernel, out_shape=outs, in_specs=[in_smem] + [in_vmem] * 5...  2.26 us
  transfers between devices with their start and end apart: 9, of which 5 were waited for; matrix products, arithmetic and copies ran while one was open for 2% of the time, Pallas kernels for 7%

profile of v2, /device:TPU:0, one launch (start us, length us, event | category | flops | bytes accessed | tf_op | source)
XLA Modules:
  0.0 104.4 jit_solution(3386929222067118760)
XLA Ops:
  0.6 8.0 %partner_low.1 = (bf16[512,2048]{1,0:T(8,128)(2,1)S(1)}, bf16[768,2048]{1,0:T(8,128)(2,1)S(1)}, bf16[1536,1024]{1,0:T(8,128)(2,1)S(1)}, bf16[1024,512]{1,0:T(8,128)(2,1)S(1)}) custom-call(s32[1]{0:T(128)} %bitcast.core.refs_0_, bf16[1536,2048]{1,0:T(8,128)(2,1)} %rows0.3, bf16[1536,1024]{1,0:T(8,128)(2,1)} %cols0.1, bf16[1536,2048]{1,0:T(8,128)(2,1)} %rows1.3, ...), custom_call_target="tpu_custom_call" | custom-call | flops 4831838208 | bytes 9437184 | tf_op jit(solution)/shard_map/partner_low/pallas_call | solution.py:167
  8.6 0.1 collective-permute-start
  8.7 5.3 %own_low.1.mine = f32[512,2048]{1,0:T(8,128)S(1)} custom-call(s32[1]{0:T(128)} %bitcast.core.refs_0_, bf16[1536,2048]{1,0:T(8,128)(2,1)} %rows0.3, bf16[1536,2048]{1,0:T(8,128)(2,1)} %rows1.3, bf16[768,2048]{1,0:T(8,128)(2,1)S(1)} %get-tuple-element.24.rows, bf16[1536,1024]{1,0:T(8,128)(2,1)S(1)} %get-tuple-element.25.cols, ...), custom_call_target="tpu_custom_call" | custom-call | flops 4831838208 | bytes 9437184 | tf_op jit(solution)/shard_map/own_low/pallas_call | solution.py:189
  14.1 1.5 %combine.1 = bf16[64,128,128]{2,1,0:T(8,128)(2,1)} custom-call(f32[512,2048]{1,0:T(8,128)S(1)} %own_low.1.mine, bf16[512,2048]{1,0:T(8,128)(2,1)S(1)} %collective-permute-done.partner), custom_call_target="tpu_custom_call" | custom-call | tf_op jit(solution)/shard_map/combine/pallas_call | solution.py:223
  15.6 14.1 %all-to-all-start = ((bf16[64,128,128]{2,1,0:T(8,128)(2,1)}), bf16[64,128,128]{2,1,0:T(8,128)(2,1)S(1)}, u32[]{:S(2)}, u32[]{:S(2)}) async-start(bf16[64,128,128]{2,1,0:T(8,128)(2,1)} %combine.1), calls=%async_computation | async-start | bytes 4194304 | tf_op jit(solution)/shard_map/all_to_all | solution.py:42
  29.8 24.8 %all-to-all-done = bf16[64,128,128]{2,1,0:T(8,128)(2,1)S(1)} async-done(((bf16[64,128,128]{2,1,0:T(8,128)(2,1)}), bf16[64,128,128]{2,1,0:T(8,128)(2,1)S(1)}, u32[]{:S(2)}, u32[]{:S(2)}) %all-to-all-start) | async-done | bytes 2097184 | tf_op jit(solution)/shard_map/all_to_all | solution.py:42
  54.6 0.3 convert_reduce_fusion.low
  54.9 0.8 moments.1
  55.8 2.8 %collective-permute-start.3 = (f32[128,128]{1,0:T(8,128)S(1)}, f32[128,128]{1,0:T(8,128)S(1)}, u32[]{:S(2)}, u32[]{:S(2)}) collective-permute-start(f32[128,128]{1,0:T(8,128)S(1)} %get-tuple-element.29.refs_0_), channel_id=1, source_target_pairs={{0,4},{2,6},{4,0},{6,2},{1,5},{3,7},{5,1},{7,3},{8,12},{10,14},{12... | collective-permute-start | bytes 196616 | tf_op jit(solution)/shard_map/ppermute | solution.py:326
  58.5 1.0 collective-permute-start.4
  59.6 1.5 %own_base.1.base = bf16[256,512]{1,0:T(8,128)(2,1)S(1)} custom-call(s32[2]{0:T(128)S(1)} %pad_add_fusion.where, bf16[2,1024,512]{2,1,0:T(8,128)(2,1)} %bases.3), custom_call_target="tpu_custom_call" | custom-call | tf_op jit(solution)/shard_map/own_base/pallas_call | solution.py:274
  61.1 0.8 collective-permute-done.2.refs_1_
  62.0 0.8 collective-permute-done.4.refs_3_
  62.8 0.9 project.1
  63.7 0.1 collective-permute-start.5
  63.8 18.2 %all_to_all.15.refs_1_ = f32[128,1,128]{2,1,0:T(1,128)S(1)} all-to-all(f32[128,1,128]{2,1,0:T(1,128)} %get-tuple-element.28), channel_id=1, replica_groups=mesh['fs_0'=4,'fs_1'=4,'tp_0'=4,'tp_1'=2] {'fs_0','fs_1','tp_0','tp_1'}, dimensions={0} | all-to-all | bytes 131072 | tf_op jit(solution)/shard_map/all_to_all | solution.py:42
  82.0 1.3 %shard_map.153 = bf16[16,2,128,128]{3,2,1,0:T(8,128)(2,1)} custom-call(s32[1]{0:T(128)} %bitcast.core.refs_0_, f32[128,1,128]{2,1,0:T(1,128)S(1)} %all_to_all.15.refs_1_, f32[128,128]{1,0:T(8,128)S(1)} %get-tuple-element.30.refs_2_, f32[128,128]{1,0:T(8,128)S(1)} %collective-permute-done.5.refs_3_, f32[128,128]{1,0:T(8,128)S(1)} %copy-done, ...), custom_call_target="tpu_custom_call" | custom-call | tf_op jit(solution)/shard_map/pallas_call | solution.py:354
  83.3 7.2 %all-to-all-start.2 = ((bf16[16,2,128,128]{3,2,1,0:T(8,128)(2,1)}), bf16[16,2,128,128]{3,2,1,0:T(8,128)(2,1)S(1)}, u32[]{:S(2)}, u32[]{:S(2)}) async-start(bf16[16,2,128,128]{3,2,1,0:T(8,128)(2,1)} %shard_map.153), calls=%async_computation.2 | async-start | bytes 2097152 | tf_op jit(solution)/shard_map/all_to_all | solution.py:42
  90.7 1.2 %collective-permute-done.6 = f32[2,64,128]{2,1,0:T(8,128)S(1)} collective-permute-done((f32[2,64,128]{2,1,0:T(8,128)S(1)}, f32[2,64,128]{2,1,0:T(8,128)S(1)}, u32[]{:S(2)}, u32[]{:S(2)}) %collective-permute-start.6) | collective-permute-done | bytes 65568 | tf_op jit(solution)/shard_map/ppermute | solution.py:48
  91.9 0.6 maximum_bitcast_fusion.1
  92.6 0.6 maximum_bitcast_fusion
  93.2 0.9 shard_map.152
  94.2 9.1 %all-to-all-done.2.gathered = bf16[16,2,128,128]{3,2,1,0:T(8,128)(2,1)S(1)} async-done(((bf16[16,2,128,128]{3,2,1,0:T(8,128)(2,1)}), bf16[16,2,128,128]{3,2,1,0:T(8,128)(2,1)S(1)}, u32[]{:S(2)}, u32[]{:S(2)}) %all-to-all-start.2) | async-done | bytes 1048608 | tf_op jit(solution)/shard_map/all_to_all | solution.py:42
  103.3 1.1 %spread.1 = (bf16[2048,128]{1,0:T(8,128)(2,1)}, bf16[128,2048]{1,0:T(8,128)(2,1)}) custom-call(bf16[16,2,128,128]{3,2,1,0:T(8,128)(2,1)S(1)} %all-to-all-done.2.gathered), custom_call_target="tpu_custom_call" | custom-call | tf_op jit(solution)/shard_map/spread/pallas_call | solution.py:374
  (22 shorter events, 0.3 us)
Async XLA Ops:
  8.6 5.4 %collective-permute-start = (bf16[512,2048]{1,0:T(8,128)(2,1)S(1)}, bf16[512,2048]{1,0:T(8,128)(2,1)S(1)}, u32[]{:S(2)}, u32[]{:S(2)}) collective-permute-start(bf16[512,2048]{1,0:T(8,128)(2,1)S(1)} %get-tuple-element.27), channel_id=1, source_target_pairs={{0,1},{1,0},{2,3},{3,2},{4,5},{5,4},{6,7},{7,6},{8,9},{9,8},{10,11... | collective-permute-start | bytes 6291464 | tf_op jit(solution)/shard_map/ppermute | solution.py:48
  15.5 14.1 %copy-start.2 = (f32[2,128,64]{1,2,0:T(8,128)S(1)}, f32[2,128,64]{1,2,0:T(8,128)}, u32[]{:S(2)}) copy-start(f32[2,128,64]{1,2,0:T(8,128)} %param.16) | copy-start | bytes 196612
  15.6 14.1 %copy-start.3 = (f32[2,128,64]{1,2,0:T(8,128)S(1)}, f32[2,128,64]{1,2,0:T(8,128)}, u32[]{:S(2)}) copy-start(f32[2,128,64]{1,2,0:T(8,128)} %param.17) | copy-start | bytes 196612
  15.6 39.1 %all-to-all-start = ((bf16[64,128,128]{2,1,0:T(8,128)(2,1)}), bf16[64,128,128]{2,1,0:T(8,128)(2,1)S(1)}, u32[]{:S(2)}, u32[]{:S(2)}) async-start(bf16[64,128,128]{2,1,0:T(8,128)(2,1)} %combine.1), calls=%async_computation | async-start | bytes 4194304 | tf_op jit(solution)/shard_map/all_to_all | solution.py:42
  29.6 52.4 %copy-start = (f32[128,128]{1,0:T(8,128)S(1)}, f32[128,128]{1,0:T(8,128)}, u32[]{:S(2)}) copy-start(f32[128,128]{1,0:T(8,128)} %refs_4_.3) | copy-start | bytes 196612
  29.6 52.4 %copy-start.1 = (f32[128,128]{1,0:T(8,128)S(1)}, f32[128,128]{1,0:T(8,128)}, u32[]{:S(2)}) copy-start(f32[128,128]{1,0:T(8,128)} %refs_5_.3) | copy-start | bytes 196612
  29.7 25.2 %collective-permute-start.1 = (f32[2,64,128]{2,1,0:T(8,128)S(1)}, f32[2,64,128]{2,1,0:T(8,128)S(1)}, u32[]{:S(2)}, u32[]{:S(2)}) collective-permute-start(f32[2,64,128]{2,1,0:T(8,128)S(1)} %pad_maximum_fusion.1), channel_id=1, source_target_pairs={{0,1},{1,0},{2,3},{3,2},{4,5},{5,4},{6,7},{7,6},{8,9},{9,8},{10,11... | collective-permute-start | bytes 196616 | tf_op jit(solution)/shard_map/ppermute | solution.py:48
  55.7 6.2 %collective-permute-start.2 = (f32[128,128]{1,0:T(8,128)S(1)}, f32[128,128]{1,0:T(8,128)S(1)}, u32[]{:S(2)}, u32[]{:S(2)}) collective-permute-start(f32[128,128]{1,0:T(8,128)S(1)} %get-tuple-element.29.refs_0_), channel_id=1, source_target_pairs={{0,2},{2,4},{4,6},{6,0},{1,3},{3,5},{5,7},{7,1},{8,10},{10,12},{12... | collective-permute-start | bytes 196616 | tf_op jit(solution)/shard_map/ppermute | solution.py:326
  55.8 6.2 %collective-permute-start.3 = (f32[128,128]{1,0:T(8,128)S(1)}, f32[128,128]{1,0:T(8,128)S(1)}, u32[]{:S(2)}, u32[]{:S(2)}) collective-permute-start(f32[128,128]{1,0:T(8,128)S(1)} %get-tuple-element.29.refs_0_), channel_id=1, source_target_pairs={{0,4},{2,6},{4,0},{6,2},{1,5},{3,7},{5,1},{7,3},{8,12},{10,14},{12... | collective-permute-start | bytes 196616 | tf_op jit(solution)/shard_map/ppermute | solution.py:326
  58.5 4.3 %collective-permute-start.4 = (f32[128,128]{1,0:T(8,128)S(1)}, f32[128,128]{1,0:T(8,128)S(1)}, u32[]{:S(2)}, u32[]{:S(2)}) collective-permute-start(f32[128,128]{1,0:T(8,128)S(1)} %get-tuple-element.29.refs_0_), channel_id=1, source_target_pairs={{0,6},{2,0},{4,2},{6,4},{1,7},{3,1},{5,3},{7,5},{8,14},{10,8},{12,... | collective-permute-start | bytes 196616 | tf_op jit(solution)/shard_map/ppermute | solution.py:326
  63.7 18.3 %collective-permute-start.5 = (f32[128,128]{1,0:T(8,128)S(1)}, f32[128,128]{1,0:T(8,128)S(1)}, u32[]{:S(2)}, u32[]{:S(2)}) collective-permute-start(f32[128,128]{1,0:T(8,128)S(1)} %get-tuple-element.31), channel_id=1, source_target_pairs={{0,1},{1,0},{2,3},{3,2},{4,5},{5,4},{6,7},{7,6},{8,9},{9,8},{10,11... | collective-permute-start | bytes 196616 | tf_op jit(solution)/shard_map/ppermute | solution.py:48
  83.3 20.0 %all-to-all-start.2 = ((bf16[16,2,128,128]{3,2,1,0:T(8,128)(2,1)}), bf16[16,2,128,128]{3,2,1,0:T(8,128)(2,1)S(1)}, u32[]{:S(2)}, u32[]{:S(2)}) async-start(bf16[16,2,128,128]{3,2,1,0:T(8,128)(2,1)} %shard_map.153), calls=%async_computation.2 | async-start | bytes 2097152 | tf_op jit(solution)/shard_map/all_to_all | solution.py:42
  90.6 1.3 %collective-permute-start.6 = (f32[2,64,128]{2,1,0:T(8,128)S(1)}, f32[2,64,128]{2,1,0:T(8,128)S(1)}, u32[]{:S(2)}, u32[]{:S(2)}) collective-permute-start(f32[2,64,128]{2,1,0:T(8,128)S(1)} %broadcast_select_fusion.2), channel_id=1, source_target_pairs={{0,1},{1,0},{2,3},{3,2},{4,5},{5,4},{6,7},{7,6},{8,9},{9,8},{10,11... | collective-permute-start | bytes 196616 | tf_op jit(solution)/shard_map/ppermute | solution.py:48

commit v3 on v2

--- a/solution.py
+++ b/solution.py
@@ -16,9 +16,9 @@
 FS_TP = ("fs_0", "fs_1", "tp_0", "tp_1")
 SWAP = [(0, 1), (1, 0)]
 LANES = 128
-CHIPS_TURN = 42
+CHIPS_TURN = 43
 SQUARES_TURN = 0
-GATHER_TURN = 10
+GATHER_TURN = 14
 MIB = 2**20
 
 
@@ -158,7 +158,7 @@
 def both_low(core, saved_input, key_cot, out_cot, mixed_out, bases):
     tokens, height = saved_input.shape
     _, width, rank = bases.shape
-    early = tokens // 2
+    early = 2 * tokens // 3
     cost = cost_of(tokens, height, width, rank)
     rows0, cols0, rows1, cols1, in_bases = (
         pltpu.with_memory_space_constraint(a, pltpu.HBM)
@@ -254,7 +254,7 @@
     return pl.pallas_call(
         moments_kernel,
         out_shape=(pltpu.VMEM(low.shape, wide),) * 3
-        + (pltpu.HBM((everyone, 1, LANES), wide),),
+        + (pltpu.VMEM((everyone, 1, LANES), wide),),
         in_specs=[in_smem] + [in_vmem] * 4,
         out_specs=(in_vmem,) * 4,
         compiler_params=pltpu.CompilerParams(vmem_limit_bytes=4 * MIB),

time: 105 us -> 103 us (0.981)
  waiting for transfers between devices: 36.9 us -> 35.7 us
  transfers between devices with their start and end apart: 9 -> 9, of which waited for: 5 -> 5; matrix products, arithmetic and copies ran while one was open for 2% -> 2% of each run, Pallas kernels for 7% -> 8%
where the time goes in v3:
time: 103 us; the launch traced here: 102 us
  waiting for transfers between devices  35.7 us (35%)
  starting transfers between devices  25.6 us (25%)
  Pallas kernels  20.8 us (20%)
  blocking collectives  17.7 us (17%)
  other arithmetic  1.69 us (2%)
    all_to_all x2, waiting for transfers between devices, exchanged(): lax.all_to_all(tiles, axes, split_axis=0, concat_axis=0, axis_index_group...  33.4 us
    all_to_all x2, starting transfers between devices, exchanged(): lax.all_to_all(tiles, axes, split_axis=0, concat_axis=0, axis_index_group...  20.8 us
    all_to_all x1, blocking collectives, exchanged(): lax.all_to_all(tiles, axes, split_axis=0, concat_axis=0, axis_index_group...  17.7 us
    pallas_call x1, Pallas kernels, both_low(): pl.pallas_call(partner_kernel, out_shape=(pltpu.VMEM((rank, height), narr...  8.04 us
    pallas_call x1, Pallas kernels, both_low(): pl.pallas_call(own_kernel, out_shape=pltpu.VMEM((rank, height), wide), in...  5.29 us
    ppermute x3, starting transfers between devices, from_others(): lax.ppermute(array, axis, [(i, (i + s) % n) for i in range(n)])  4.44 us
    pallas_call x2, Pallas kernels, stepped(): pl.pallas_call(kernel, out_shape=outs, in_specs=[in_smem] + [in_vmem] * 5...  2.26 us
  transfers between devices with their start and end apart: 9, of which 5 were waited for; matrix products, arithmetic and copies ran while one was open for 2% of the time, Pallas kernels for 8%

profile of v3, /device:TPU:0, one launch (start us, length us, event | category | flops | bytes accessed | tf_op | source)
XLA Modules:
  0.0 102.3 jit_solution(14647084556132959173)
XLA Ops:
  0.6 8.0 %partner_low.1 = (bf16[512,2048]{1,0:T(8,128)(2,1)S(1)}, bf16[1024,2048]{1,0:T(8,128)(2,1)S(1)}, bf16[1536,1024]{1,0:T(8,128)(2,1)S(1)}, bf16[1024,512]{1,0:T(8,128)(2,1)S(1)}) custom-call(s32[1]{0:T(128)} %bitcast.core.refs_0_, bf16[1536,2048]{1,0:T(8,128)(2,1)} %rows0.3, bf16[1536,1024]{1,0:T(8,128)(2,1)} %cols0.1, bf16[1536,2048]{1,0:T(8,128)(2,1)} %rows1.3, ...), custom_call_target="tpu_custom_call" | custom-call | flops 4831838208 | bytes 9437184 | tf_op jit(solution)/shard_map/partner_low/pallas_call | solution.py:167
  8.7 0.1 collective-permute-start
  8.8 5.3 %own_low.1.mine = f32[512,2048]{1,0:T(8,128)S(1)} custom-call(s32[1]{0:T(128)} %bitcast.core.refs_0_, bf16[1536,2048]{1,0:T(8,128)(2,1)} %rows0.3, bf16[1536,2048]{1,0:T(8,128)(2,1)} %rows1.3, bf16[1024,2048]{1,0:T(8,128)(2,1)S(1)} %get-tuple-element.24.rows, bf16[1536,1024]{1,0:T(8,128)(2,1)S(1)} %get-tuple-element.25.cols, ...), custom_call_target="tpu_custom_call" | custom-call | flops 4831838208 | bytes 9437184 | tf_op jit(solution)/shard_map/own_low/pallas_call | solution.py:189
  14.1 1.5 %combine.1 = bf16[64,128,128]{2,1,0:T(8,128)(2,1)} custom-call(f32[512,2048]{1,0:T(8,128)S(1)} %own_low.1.mine, bf16[512,2048]{1,0:T(8,128)(2,1)S(1)} %collective-permute-done.partner), custom_call_target="tpu_custom_call" | custom-call | tf_op jit(solution)/shard_map/combine/pallas_call | solution.py:223
  15.6 13.8 %all-to-all-start = ((bf16[64,128,128]{2,1,0:T(8,128)(2,1)}), bf16[64,128,128]{2,1,0:T(8,128)(2,1)S(1)}, u32[]{:S(2)}, u32[]{:S(2)}) async-start(bf16[64,128,128]{2,1,0:T(8,128)(2,1)} %combine.1), calls=%async_computation | async-start | bytes 4194304 | tf_op jit(solution)/shard_map/all_to_all | solution.py:42
  29.6 24.9 %all-to-all-done = bf16[64,128,128]{2,1,0:T(8,128)(2,1)S(1)} async-done(((bf16[64,128,128]{2,1,0:T(8,128)(2,1)}), bf16[64,128,128]{2,1,0:T(8,128)(2,1)S(1)}, u32[]{:S(2)}, u32[]{:S(2)}) %all-to-all-start) | async-done | bytes 2097184 | tf_op jit(solution)/shard_map/all_to_all | solution.py:42
  54.5 0.3 convert_reduce_fusion.low
  54.8 0.2 moments.1
  55.0 0.4 collective-permute-start.2
  55.5 2.3 %collective-permute-start.3 = (f32[128,128]{1,0:T(8,128)S(1)}, f32[128,128]{1,0:T(8,128)S(1)}, u32[]{:S(2)}, u32[]{:S(2)}) collective-permute-start(f32[128,128]{1,0:T(8,128)S(1)} %get-tuple-element.29.refs_0_), channel_id=1, source_target_pairs={{0,4},{2,6},{4,0},{6,2},{1,5},{3,7},{5,1},{7,3},{8,12},{10,14},{12... | collective-permute-start | bytes 196616 | tf_op jit(solution)/shard_map/ppermute | solution.py:326
  57.8 1.7 %collective-permute-start.4 = (f32[128,128]{1,0:T(8,128)S(1)}, f32[128,128]{1,0:T(8,128)S(1)}, u32[]{:S(2)}, u32[]{:S(2)}) collective-permute-start(f32[128,128]{1,0:T(8,128)S(1)} %get-tuple-element.29.refs_0_), channel_id=1, source_target_pairs={{0,6},{2,0},{4,2},{6,4},{1,7},{3,1},{5,3},{7,5},{8,14},{10,8},{12,... | collective-permute-start | bytes 196616 | tf_op jit(solution)/shard_map/ppermute | solution.py:326
  59.5 1.5 %own_base.1.base = bf16[256,512]{1,0:T(8,128)(2,1)S(1)} custom-call(s32[2]{0:T(128)S(1)} %pad_add_fusion.where, bf16[2,1024,512]{2,1,0:T(8,128)(2,1)} %bases.3), custom_call_target="tpu_custom_call" | custom-call | tf_op jit(solution)/shard_map/own_base/pallas_call | solution.py:274
  61.0 0.2 collective-permute-done.2.refs_1_
  61.3 0.9 collective-permute-done.4.refs_3_
  62.1 0.9 project.1
  63.1 17.7 %all_to_all.15.refs_1_ = f32[128,1,128]{2,1,0:T(1,128)S(1)} all-to-all(f32[128,1,128]{2,1,0:T(1,128)S(1)} %get-tuple-element.28), channel_id=1, replica_groups=mesh['fs_0'=4,'fs_1'=4,'tp_0'=4,'tp_1'=2] {'fs_0','fs_1','tp_0','tp_1'}, dimensions={0} | all-to-all | bytes 131072 | tf_op jit(solution)/shard_map/all_to_all | solution.py:42
  80.8 1.3 %shard_map.153 = bf16[16,2,128,128]{3,2,1,0:T(8,128)(2,1)} custom-call(s32[1]{0:T(128)} %bitcast.core.refs_0_, f32[128,1,128]{2,1,0:T(1,128)S(1)} %all_to_all.15.refs_1_, f32[128,128]{1,0:T(8,128)S(1)} %get-tuple-element.30.refs_2_, f32[128,128]{1,0:T(8,128)S(1)} %collective-permute-done.5.refs_3_, f32[128,128]{1,0:T(8,128)S(1)} %copy-done, ...), custom_call_target="tpu_custom_call" | custom-call | tf_op jit(solution)/shard_map/pallas_call | solution.py:354
  82.1 7.0 %all-to-all-start.2 = ((bf16[16,2,128,128]{3,2,1,0:T(8,128)(2,1)}), bf16[16,2,128,128]{3,2,1,0:T(8,128)(2,1)S(1)}, u32[]{:S(2)}, u32[]{:S(2)}) async-start(bf16[16,2,128,128]{3,2,1,0:T(8,128)(2,1)} %shard_map.153), calls=%async_computation.2 | async-start | bytes 2097152 | tf_op jit(solution)/shard_map/all_to_all | solution.py:42
  89.2 1.2 %collective-permute-done.6 = f32[2,64,128]{2,1,0:T(8,128)S(1)} collective-permute-done((f32[2,64,128]{2,1,0:T(8,128)S(1)}, f32[2,64,128]{2,1,0:T(8,128)S(1)}, u32[]{:S(2)}, u32[]{:S(2)}) %collective-permute-start.6) | collective-permute-done | bytes 65568 | tf_op jit(solution)/shard_map/ppermute | solution.py:48
  90.5 0.6 maximum_bitcast_fusion.1
  91.1 0.6 maximum_bitcast_fusion
  91.8 0.9 shard_map.152
  92.7 8.5 %all-to-all-done.2.gathered = bf16[16,2,128,128]{3,2,1,0:T(8,128)(2,1)S(1)} async-done(((bf16[16,2,128,128]{3,2,1,0:T(8,128)(2,1)}), bf16[16,2,128,128]{3,2,1,0:T(8,128)(2,1)S(1)}, u32[]{:S(2)}, u32[]{:S(2)}) %all-to-all-start.2) | async-done | bytes 1048608 | tf_op jit(solution)/shard_map/all_to_all | solution.py:42
  101.2 1.1 %spread.1 = (bf16[2048,128]{1,0:T(8,128)(2,1)}, bf16[128,2048]{1,0:T(8,128)(2,1)}) custom-call(bf16[16,2,128,128]{3,2,1,0:T(8,128)(2,1)S(1)} %all-to-all-done.2.gathered), custom_call_target="tpu_custom_call" | custom-call | tf_op jit(solution)/shard_map/spread/pallas_call | solution.py:374
  (22 shorter events, 0.4 us)
Async XLA Ops:
  8.7 5.4 %collective-permute-start = (bf16[512,2048]{1,0:T(8,128)(2,1)S(1)}, bf16[512,2048]{1,0:T(8,128)(2,1)S(1)}, u32[]{:S(2)}, u32[]{:S(2)}) collective-permute-start(bf16[512,2048]{1,0:T(8,128)(2,1)S(1)} %get-tuple-element.27), channel_id=1, source_target_pairs={{0,1},{1,0},{2,3},{3,2},{4,5},{5,4},{6,7},{7,6},{8,9},{9,8},{10,11... | collective-permute-start | bytes 6291464 | tf_op jit(solution)/shard_map/ppermute | solution.py:48
  15.6 13.9 %copy-start.2 = (f32[2,128,64]{1,2,0:T(8,128)S(1)}, f32[2,128,64]{1,2,0:T(8,128)}, u32[]{:S(2)}) copy-start(f32[2,128,64]{1,2,0:T(8,128)} %param.16) | copy-start | bytes 196612
  15.6 13.9 %copy-start.3 = (f32[2,128,64]{1,2,0:T(8,128)S(1)}, f32[2,128,64]{1,2,0:T(8,128)}, u32[]{:S(2)}) copy-start(f32[2,128,64]{1,2,0:T(8,128)} %param.17) | copy-start | bytes 196612
  15.6 38.9 %all-to-all-start = ((bf16[64,128,128]{2,1,0:T(8,128)(2,1)}), bf16[64,128,128]{2,1,0:T(8,128)(2,1)S(1)}, u32[]{:S(2)}, u32[]{:S(2)}) async-start(bf16[64,128,128]{2,1,0:T(8,128)(2,1)} %combine.1), calls=%async_computation | async-start | bytes 4194304 | tf_op jit(solution)/shard_map/all_to_all | solution.py:42
  29.4 51.4 %copy-start = (f32[128,128]{1,0:T(8,128)S(1)}, f32[128,128]{1,0:T(8,128)}, u32[]{:S(2)}) copy-start(f32[128,128]{1,0:T(8,128)} %refs_4_.3) | copy-start | bytes 196612
  29.4 51.4 %copy-start.1 = (f32[128,128]{1,0:T(8,128)S(1)}, f32[128,128]{1,0:T(8,128)}, u32[]{:S(2)}) copy-start(f32[128,128]{1,0:T(8,128)} %refs_5_.3) | copy-start | bytes 196612
  29.5 25.3 %collective-permute-start.1 = (f32[2,64,128]{2,1,0:T(8,128)S(1)}, f32[2,64,128]{2,1,0:T(8,128)S(1)}, u32[]{:S(2)}, u32[]{:S(2)}) collective-permute-start(f32[2,64,128]{2,1,0:T(8,128)S(1)} %pad_maximum_fusion.1), channel_id=1, source_target_pairs={{0,1},{1,0},{2,3},{3,2},{4,5},{5,4},{6,7},{7,6},{8,9},{9,8},{10,11... | collective-permute-start | bytes 196616 | tf_op jit(solution)/shard_map/ppermute | solution.py:48
  55.0 6.2 %collective-permute-start.2 = (f32[128,128]{1,0:T(8,128)S(1)}, f32[128,128]{1,0:T(8,128)S(1)}, u32[]{:S(2)}, u32[]{:S(2)}) collective-permute-start(f32[128,128]{1,0:T(8,128)S(1)} %get-tuple-element.29.refs_0_), channel_id=1, source_target_pairs={{0,2},{2,4},{4,6},{6,0},{1,3},{3,5},{5,7},{7,1},{8,10},{10,12},{12... | collective-permute-start | bytes 196616 | tf_op jit(solution)/shard_map/ppermute | solution.py:326
  55.5 5.8 %collective-permute-start.3 = (f32[128,128]{1,0:T(8,128)S(1)}, f32[128,128]{1,0:T(8,128)S(1)}, u32[]{:S(2)}, u32[]{:S(2)}) collective-permute-start(f32[128,128]{1,0:T(8,128)S(1)} %get-tuple-element.29.refs_0_), channel_id=1, source_target_pairs={{0,4},{2,6},{4,0},{6,2},{1,5},{3,7},{5,1},{7,3},{8,12},{10,14},{12... | collective-permute-start | bytes 196616 | tf_op jit(solution)/shard_map/ppermute | solution.py:326
  57.8 4.3 %collective-permute-start.4 = (f32[128,128]{1,0:T(8,128)S(1)}, f32[128,128]{1,0:T(8,128)S(1)}, u32[]{:S(2)}, u32[]{:S(2)}) collective-permute-start(f32[128,128]{1,0:T(8,128)S(1)} %get-tuple-element.29.refs_0_), channel_id=1, source_target_pairs={{0,6},{2,0},{4,2},{6,4},{1,7},{3,1},{5,3},{7,5},{8,14},{10,8},{12,... | collective-permute-start | bytes 196616 | tf_op jit(solution)/shard_map/ppermute | solution.py:326
  63.0 17.8 %collective-permute-start.5 = (f32[128,128]{1,0:T(8,128)S(1)}, f32[128,128]{1,0:T(8,128)S(1)}, u32[]{:S(2)}, u32[]{:S(2)}) collective-permute-start(f32[128,128]{1,0:T(8,128)S(1)} %get-tuple-element.31), channel_id=1, source_target_pairs={{0,1},{1,0},{2,3},{3,2},{4,5},{5,4},{6,7},{7,6},{8,9},{9,8},{10,11... | collective-permute-start | bytes 196616 | tf_op jit(solution)/shard_map/ppermute | solution.py:48
  82.1 19.0 %all-to-all-start.2 = ((bf16[16,2,128,128]{3,2,1,0:T(8,128)(2,1)}), bf16[16,2,128,128]{3,2,1,0:T(8,128)(2,1)S(1)}, u32[]{:S(2)}, u32[]{:S(2)}) async-start(bf16[16,2,128,128]{3,2,1,0:T(8,128)(2,1)} %shard_map.153), calls=%async_computation.2 | async-start | bytes 2097152 | tf_op jit(solution)/shard_map/all_to_all | solution.py:42
  89.1 1.3 %collective-permute-start.6 = (f32[2,64,128]{2,1,0:T(8,128)S(1)}, f32[2,64,128]{2,1,0:T(8,128)S(1)}, u32[]{:S(2)}, u32[]{:S(2)}) collective-permute-start(f32[2,64,128]{2,1,0:T(8,128)S(1)} %broadcast_select_fusion.2), channel_id=1, source_target_pairs={{0,1},{1,0},{2,3},{3,2},{4,5},{5,4},{6,7},{7,6},{8,9},{9,8},{10,11... | collective-permute-start | bytes 196616 | tf_op jit(solution)/shard_map/ppermute | solution.py:48
